TPU v7x, 512 devices: a whole 4x4x16 slice. The times are simulated.
512 devices in a mesh: ep: 32 (over z, core), tp: 16 (over y, x).
Axes of the slice: x: 4, y: 4, z: 16, core: 2. Of those that a mesh axis runs over, the one named last changes fastest.
Arguments:
- tokens: bfloat16 [1024, 4096], P('ep'), may hold values from -6 to 6
- recur_state: float32 [1024, 4096], P('ep', 'tp'), may hold values from -6 to 6
- conv_state: bfloat16 [1024, 3, 4096], P('ep', None, 'tp'), may hold values from -6 to 6
- mix_gain: float32 [4096], replicated, may hold values from 0.1 to 1.9
- in_weight: bfloat16 [4096, 4096], P('ep', 'tp'), may hold values from -0.09375 to 0.09375
- gate_weight: bfloat16 [4096, 4096], P('ep', 'tp'), may hold values from -0.09375 to 0.09375
- conv_taps: float32 [4, 4096], P(None, 'tp'), may hold values from -3 to 3
- recur_gate_blocks: bfloat16 [64, 64, 64], P('tp'), may hold values from -0.75 to 0.75
- input_gate_blocks: bfloat16 [64, 64, 64], P('tp'), may hold values from -0.75 to 0.75
- decay_rate: float32 [4096], P('tp'), may hold values from 0.01 to 0.4
- out_weight: bfloat16 [4096, 4096], P('tp', 'ep'), may hold values from -0.09375 to 0.09375
- ffn_gain: float32 [4096], replicated, may hold values from 0.1 to 1.9
- router_weight: bfloat16 [4096, 32], replicated, may hold values from -0.09375 to 0.09375
- routes: int32 [1024, 2], P('ep'), may hold values from 0 to 31, as said below
- expert_gate: bfloat16 [32, 4096, 2048], P('ep', None, 'tp'), may hold values from -0.09375 to 0.09375
- expert_up: bfloat16 [32, 4096, 2048], P('ep', None, 'tp'), may hold values from -0.09375 to 0.09375
- expert_down: bfloat16 [32, 2048, 4096], P('ep', 'tp'), may hold values from -0.125 to 0.125
- dense_gate: bfloat16 [4096, 2048], P('ep', 'tp'), may hold values from -0.09375 to 0.09375
- dense_up: bfloat16 [4096, 2048], P('ep', 'tp'), may hold values from -0.09375 to 0.09375
- dense_down: bfloat16 [2048, 4096], P('tp', 'ep'), may hold values from -0.125 to 0.125
- branch_gate: bfloat16 [4096], replicated, may hold values from -0.09375 to 0.09375
Outputs:
- layer_out: bfloat16 [1024, 4096], P('ep')
- new_state: float32 [1024, 4096], P('ep', 'tp')
- new_conv_state: bfloat16 [1024, 3, 4096], P('ep', None, 'tp')
Inputs may be any that keep to these rules, and one draw needn't show every extreme that they name: `routes`: A row names two different experts of one group: both have the same e // 4. In the rows of one index of ep no expert is named more than 4 times, and in every draw some expert is named exactly 4 times by the rows of every index of ep.
All inputs are finite; a program needn't handle non-finite values.
Results may differ from a plain program's by a relative error of at most 0.023.
Values may be sent and summed in bfloat16 or wider, within the bound.
No kernel may reach another device: no remote copies, remote signals or barrier semaphores. Data moves between devices by JAX's collectives and lax.ppermute only.
A program may use at most 64 MiB of HBM per device.

v0:
```python
import jax
import jax.numpy as jnp
from jax import lax
from jax.sharding import Mesh
from jax.sharding import PartitionSpec as P

TOP_K = 2
EP = ("ep_0", "ep_1")


epsilon = 1e-06
decay_scale = 8.0


def side_by_side(arrays, axis, dim, along):
    ends, at = ([], 0)
    for a in arrays[:-1]:
        at += a.shape[along]
        ends.append(at)
    both = jnp.concatenate(arrays, axis=along)
    return tuple(jnp.split(lax.all_gather(both, axis, axis=dim, tiled=True), ends, axis=along))


def copy_for_each(value, axis):
    copies = jnp.broadcast_to(value, (lax.axis_size(axis), *value.shape))
    return lax.all_to_all(copies, axis, split_axis=0, concat_axis=0, tiled=True)


def joined_along(pieces, dim):
    pieces = jnp.moveaxis(pieces, 0, dim)
    shape = pieces.shape
    return pieces.reshape(*shape[:dim], shape[dim] * shape[dim + 1], *shape[dim + 2 :])


def whole_of(value, axes, dim):
    far, near = axes
    pieces = copy_for_each(copy_for_each(value, far), near)
    return joined_along(pieces.swapaxes(0, 1).reshape(-1, *value.shape), dim)


def cut_along(value, dim, devices):
    before, after = (value.shape[:dim], value.shape[dim + 1 :])
    return jnp.moveaxis(value.reshape(*before, devices, -1, *after), dim, 0)


def summed_on_arrival(value, axis, dim):
    pieces = cut_along(value, dim, lax.axis_size(axis))
    arrived = lax.all_to_all(pieces, axis, split_axis=0, concat_axis=0, tiled=True)
    return arrived.astype(jnp.float32).sum(axis=0)


def rows_for(lines, devices):
    spare = -lines.shape[0] % devices
    if not spare:
        return lines
    return jnp.concatenate([lines, jnp.zeros((spare, *lines.shape[1:]), lines.dtype)])


def gathered_copies(value, axis, dim):
    pieces = copy_for_each(value, axis)
    return joined_along(pieces, dim)


def sum_by_parts(value, axes):
    lines = value.reshape(-1, value.shape[-1])
    own = summed_on_arrival(rows_for(lines, lax.axis_size(axes)), axes, 0)
    whole = gathered_copies(own.astype(jnp.bfloat16), axes, 0)
    return whole[: len(lines)].reshape(value.shape).astype(jnp.float32)


def all_blocks(value, axes, turns):
    pieces = value
    for k in turns:
        pieces = lax.all_gather(pieces, axes[k])
    done = turns[::-1]
    back = [done.index(k) for k in range(len(axes))]
    pieces = pieces.transpose(*back, *range(len(axes), pieces.ndim))
    return pieces.reshape(-1, *value.shape)


def gathered_by_axis(value, axes, turns, dim):
    return joined_along(all_blocks(value, axes, turns), dim)


def rms_scale(rows, gain):
    values = rows.astype(jnp.float32)
    inverse = lax.rsqrt(jnp.mean(values * values, axis=-1, keepdims=True) + epsilon)
    return (values * inverse * gain).astype(jnp.bfloat16)


def fold_pair(source, pieces):
    return (
        jnp.dot(source, pieces[0], preferred_element_type=jnp.float32),
        jnp.dot(source, pieces[1], preferred_element_type=jnp.float32),
    )


def on_device(
    tokens,
    recur_state,
    conv_state,
    mix_gain,
    in_weight,
    gate_weight,
    conv_taps,
    recur_gate_blocks,
    input_gate_blocks,
    decay_rate,
    out_weight,
    ffn_gain,
    router_weight,
    routes,
    expert_gate,
    expert_up,
    expert_down,
    dense_gate,
    dense_up,
    dense_down,
    branch_gate,
):
    batch_rows, width = tokens.shape
    channels = in_weight.shape[1]
    normed = rms_scale(tokens, mix_gain)
    x_sum, gate_sum = fold_pair(normed, side_by_side((in_weight, gate_weight), EP, 0, 1))
    x_branch = x_sum.astype(jnp.bfloat16)
    gate_branch = gate_sum.astype(jnp.bfloat16)
    window = jnp.concatenate([conv_state, x_branch[:, None, :]], axis=1)
    conv_out = jnp.sum(window.astype(jnp.float32) * conv_taps[None], axis=1).astype(jnp.bfloat16)
    new_conv_state = window[:, 1:, :]
    blocks = conv_out.reshape(batch_rows, recur_gate_blocks.shape[0], recur_gate_blocks.shape[1])
    recur_gate = jax.nn.sigmoid(
        jnp.einsum(
            "bhi,hij->bhj", blocks, recur_gate_blocks, preferred_element_type=jnp.float32
        ).reshape(batch_rows, channels)
    )
    input_gate = jax.nn.sigmoid(
        jnp.einsum(
            "bhi,hij->bhj", blocks, input_gate_blocks, preferred_element_type=jnp.float32
        ).reshape(batch_rows, channels)
    )
    log_decay = -decay_scale * recur_gate * decay_rate
    new_state = jnp.exp(log_decay) * recur_state + jnp.sqrt(
        -jnp.expm1(2.0 * log_decay)
    ) * input_gate * conv_out.astype(jnp.float32)
    mixer_rows = (new_state * jax.nn.gelu(gate_branch.astype(jnp.float32))).astype(jnp.bfloat16)
    mixer_part = jnp.dot(
        mixer_rows, whole_of(out_weight, ("ep_0", "ep_1"), 1), preferred_element_type=jnp.float32
    )
    resid = (
        tokens.astype(jnp.float32) + sum_by_parts(mixer_part.astype(jnp.bfloat16), "tp")
    ).astype(jnp.bfloat16)
    normed_ffn = rms_scale(resid, ffn_gain)
    router_logits = jnp.dot(normed_ffn, router_weight, preferred_element_type=jnp.float32)
    experts = router_logits.shape[1]
    expert_ids = lax.broadcasted_iota(jnp.int32, (batch_rows, TOP_K, experts), 2)
    picked = jnp.sum(
        jnp.where(routes[:, :, None] == expert_ids, router_logits[:, None, :], 0.0), axis=2
    )
    route_weight = jax.nn.sigmoid(picked - picked[:, ::-1]).astype(jnp.bfloat16)
    capacity = 2 * batch_rows * TOP_K // experts
    flat_ids = routes.reshape(batch_rows * TOP_K)
    onehot = (
        flat_ids[:, None] == lax.broadcasted_iota(jnp.int32, (batch_rows * TOP_K, experts), 1)
    ).astype(jnp.int32)
    rank = jnp.sum((jnp.cumsum(onehot, axis=0) - onehot) * onehot, axis=1)
    slot_of = (flat_ids * capacity + rank).reshape(batch_rows, TOP_K)
    slot_rows = lax.broadcasted_iota(jnp.int32, (experts * capacity, batch_rows), 0)
    slot_cols = lax.broadcasted_iota(jnp.int32, (batch_rows, experts * capacity), 1)
    dispatch = jnp.zeros((experts * capacity, batch_rows), jnp.bfloat16)
    combine = jnp.zeros((batch_rows, experts * capacity), jnp.bfloat16)
    for pick in range(TOP_K):
        dispatch = dispatch + (slot_rows == slot_of[None, :, pick]).astype(jnp.bfloat16)
        combine = combine + jnp.where(
            slot_cols == slot_of[:, pick : pick + 1],
            route_weight[:, pick : pick + 1],
            jnp.zeros((), jnp.bfloat16),
        )
    outgoing = (
        jnp.dot(dispatch, normed_ffn, preferred_element_type=jnp.float32)
        .astype(jnp.bfloat16)
        .reshape(experts, capacity, width)
    )
    gate_local = expert_gate[0]
    up_local = expert_up[0]
    down_local = expert_down[0]
    arrived_rows = lax.all_to_all(outgoing, EP, split_axis=0, concat_axis=0, tiled=True)
    sources, items, features = arrived_rows.shape
    rows = arrived_rows.reshape(sources * items, features)
    first = jnp.dot(rows, gate_local, preferred_element_type=jnp.float32)
    second = jnp.dot(rows, up_local, preferred_element_type=jnp.float32)
    act = (jax.nn.silu(first) * second).astype(jnp.bfloat16)
    partial_value = jnp.dot(act, down_local, preferred_element_type=jnp.float32)
    total = summed_on_arrival(partial_value.astype(jnp.bfloat16), "tp", 1).astype(jnp.bfloat16)
    returned = lax.all_to_all(
        total.reshape(sources, items, total.shape[1]), EP, split_axis=0, concat_axis=0, tiled=True
    )
    moe = jnp.dot(
        combine,
        returned.reshape(experts * capacity, returned.shape[2]),
        preferred_element_type=jnp.float32,
    )
    dense_first, dense_second = fold_pair(
        normed_ffn, side_by_side((dense_gate, dense_up), EP, 0, 1)
    )
    dense_act = (jax.nn.silu(dense_first) * dense_second).astype(jnp.bfloat16)
    dense_part = jnp.dot(
        dense_act, gathered_by_axis(dense_down, EP, (0, 1), 1), preferred_element_type=jnp.float32
    )
    branch_weight = jax.nn.sigmoid(
        jnp.dot(normed_ffn, branch_gate, preferred_element_type=jnp.float32)
    )
    share = moe.shape[1]
    offset = lax.axis_index("tp") * share
    resid_share = lax.dynamic_slice_in_dim(resid, offset, share, 1).astype(jnp.float32)
    dense_share = summed_on_arrival(dense_part.astype(jnp.bfloat16), "tp", 1)
    out_share = (resid_share + moe + branch_weight[:, None] * dense_share).astype(jnp.bfloat16)
    layer_out = gathered_copies(out_share, "tp", 1)
    return (layer_out, new_state, new_conv_state)


def solution(mesh):
    split = Mesh(mesh.devices.reshape(16, 2, mesh.shape["tp"]), ("ep_0", "ep_1", "tp"))
    in_specs = (
        P(EP, None),
        P(EP, "tp"),
        P(EP, None, "tp"),
        P(),
        P(EP, "tp"),
        P(EP, "tp"),
        P(None, "tp"),
        P("tp", None, None),
        P("tp", None, None),
        P("tp"),
        P("tp", EP),
        P(),
        P(),
        P(EP, None),
        P(EP, None, "tp"),
        P(EP, None, "tp"),
        P(EP, "tp", None),
        P(EP, "tp"),
        P(EP, "tp"),
        P("tp", EP),
        P(),
    )
    out_specs = (P(EP, None), P(EP, "tp"), P(EP, None, "tp"))
    return jax.shard_map(
        on_device, mesh=split, in_specs=in_specs, out_specs=out_specs, check_vma=False
    )
```

profile of v0, /device:TPU:1, one launch (start us, length us, event | category | flops | bytes accessed | tf_op | source)
XLA Modules:
  0.0 327.2 jit_solution(10356906734136988550)
XLA Ops:
  7.2 1.6 pad_maximum_fusion
  8.9 2.1 broadcast_in_dim.59
  11.0 15.7 %all-to-all-start = ((bf16[16,256,128]{2,1,0:T(8,128)(2,1)}), bf16[16,256,128]{2,1,0:T(8,128)(2,1)S(1)}, u32[]{:S(2)}, u32[]{:S(2)}) async-start(bf16[16,256,128]{2,1,0:T(8,128)(2,1)} %broadcast_in_dim.59), calls=%async_computation | async-start | bytes 2097152 | tf_op jit(solution)/shard_map/all_to_all | solution.py:26
  26.8 82.2 %all-gather = bf16[2048,128]{1,0:T(8,128)(2,1)} all-gather(bf16[128,128]{1,0:T(8,128)(2,1)S(1)} %copy-done.7), channel_id=2, replica_groups=mesh['ep_0'=16,'ep_1'=2,'tp'=16] {'ep_0'}, dimensions={0}, use_global_device_ids=true | all-gather | bytes 557056 | tf_op jit(solution)/shard_map/all_gather | solution.py:74
  109.1 0.6 eq.54
  109.9 0.5 broadcast_multiply_fusion
  110.9 12.7 %all_to_all.45 = bf16[2,16,256,128]{3,2,1,0:T(8,128)(2,1)S(1)} all-to-all(bf16[2,16,256,128]{3,2,1,0:T(8,128)(2,1)S(1)} %broadcast_in_dim.60), channel_id=1, replica_groups=mesh['ep_0'=16,'ep_1'=2,'tp'=16] {'ep_1'}, dimensions={0} | all-to-all | bytes 4194304 | tf_op jit(solution)/shard_map/all_to_all | solution.py:26
  123.6 1.5 copy.98
  125.1 3.3 %copy.99 = bf16[256,32,128]{0,2,1:T(8,128)(2,1)S(1)} copy(bf16[256,32,128]{2,0,1:T(8,128)(2,1)} %bitcast.75) | data formatting | bytes 4194304 | tf_op jit(solution)/shard_map/transpose | solution.py:30
  128.5 2.1 fusion.24
  130.8 0.6 copy-done.8
  131.4 1.0 fusion.7
  132.4 0.7 div.36
  133.1 1.0 fusion.11
  134.2 0.7 div.34
  134.9 0.8 multiply_add_fusion
  135.8 3.9 %convolution_convert_fusion.3 = bf16[32,4096]{1,0:T(8,128)(2,1)} fusion(bf16[256,4096]{0,1:T(8,128)(2,1)S(1)} %bitcast.74, f32[32,256]{1,0:T(8,128)S(1)} %multiply_add_fusion, bf16[4096,512]{1,0:T(8,128)(2,1)} %all-gather.6.cloned.1.call-done, bf16[32,4096]{1,0:T(8,128)(2,1)S(1)} %copy-done.1, f32[4096]{0:T(1024)} %param.24, f32[32]{0:T(128)} %copy-done.19), kind=kOutput, calls=%fused_computation.3 | convolution fusion | flops 134971392 | bytes 4768256 | tf_op jit(solution)/shard_map/dot_general | solution.py:146
  139.7 1.8 reshape.93
  141.6 6.9 %all-to-all-start.2 = ((bf16[16,2,4096]{2,1,0:T(2,128)(2,1)}), bf16[16,2,4096]{2,1,0:T(2,128)(2,1)S(1)}, u32[]{:S(2)}, u32[]{:S(2)}) async-start(bf16[16,2,4096]{2,1,0:T(2,128)(2,1)} %reshape.93), calls=%async_computation.2 | async-start | bytes 524288 | tf_op jit(solution)/shard_map/all_to_all | solution.py:48
  149.0 7.6 %all-to-all-done.2 = bf16[16,2,4096]{2,1,0:T(2,128)(2,1)S(1)} async-done(((bf16[16,2,4096]{2,1,0:T(2,128)(2,1)}), bf16[16,2,4096]{2,1,0:T(2,128)(2,1)S(1)}, u32[]{:S(2)}, u32[]{:S(2)}) %all-to-all-start.2) | async-done | bytes 262176 | tf_op jit(solution)/shard_map/all_to_all | solution.py:48
  156.8 0.9 broadcast_in_dim.61
  157.7 3.5 %all-to-all-start.3 = ((bf16[16,2,4096]{2,1,0:T(2,128)(2,1)}), bf16[16,2,4096]{2,1,0:T(2,128)(2,1)S(1)}, u32[]{:S(2)}, u32[]{:S(2)}) async-start(bf16[16,2,4096]{2,1,0:T(2,128)(2,1)} %broadcast_in_dim.61), calls=%async_computation.3 | async-start | bytes 524288 | tf_op jit(solution)/shard_map/all_to_all | solution.py:26
  161.3 7.5 %all-to-all-done.3 = bf16[16,2,4096]{2,1,0:T(2,128)(2,1)S(1)} async-done(((bf16[16,2,4096]{2,1,0:T(2,128)(2,1)}), bf16[16,2,4096]{2,1,0:T(2,128)(2,1)S(1)}, u32[]{:S(2)}, u32[]{:S(2)}) %all-to-all-start.3) | async-done | bytes 262176 | tf_op jit(solution)/shard_map/all_to_all | solution.py:26
  169.6 1.2 reshape.94
  170.8 11.5 %all-to-all-start.4 = ((bf16[32,4,4096]{2,1,0:T(4,128)(2,1)}), bf16[32,4,4096]{2,1,0:T(4,128)(2,1)S(1)}, u32[]{:S(2)}, u32[]{:S(2)}) async-start(bf16[32,4,4096]{2,1,0:T(4,128)(2,1)} %reshape.94), calls=%async_computation.4 | async-start | bytes 2097152 | tf_op jit(solution)/shard_map/all_to_all | solution.py:186
  182.4 0.6 pad_maximum_fusion.2
  183.0 58.6 %all-to-all-done.4 = bf16[32,4,4096]{2,1,0:T(4,128)(2,1)S(1)} async-done(((bf16[32,4,4096]{2,1,0:T(4,128)(2,1)}), bf16[32,4,4096]{2,1,0:T(4,128)(2,1)S(1)}, u32[]{:S(2)}, u32[]{:S(2)}) %all-to-all-start.4) | async-done | bytes 1048608 | tf_op jit(solution)/shard_map/all_to_all | solution.py:186
  241.9 1.7 fusion.39
  243.6 2.0 convolution_convert_fusion
  245.6 1.1 copy.116
  246.7 3.7 %all-to-all-start.5 = ((bf16[16,128,256]{2,1,0:T(8,128)(2,1)}), bf16[16,128,256]{2,1,0:T(8,128)(2,1)S(1)}, u32[]{:S(2)}, u32[]{:S(2)}) async-start(bf16[16,128,256]{2,1,0:T(8,128)(2,1)} %bitcast.71), calls=%async_computation.5 | async-start | bytes 2097152 | tf_op jit(solution)/shard_map/all_to_all | solution.py:48
  250.5 2.4 copy.103
  252.8 1.6 copy.104
  254.4 9.9 %all-gather.8.cloned.1.call-done = bf16[4096,256]{1,0:T(8,128)(2,1)} async-done(((bf16[128,256]{1,0:T(8,128)(2,1)}), bf16[4096,256]{1,0:T(8,128)(2,1)}) %all-gather.8.cloned.1.call-update) | async-done | bytes 2097168 | tf_op jit(solution)/shard_map/all_gather | solution.py:21
  264.4 1.5 fusion.34
  265.9 2.7 convolution_convert_fusion.2
  268.6 1.7 copy.117
  270.3 1.2 fusion.125
  271.7 6.7 %all-to-all-start.7 = ((bf16[16,32,256]{2,1,0:T(8,128)(2,1)}), bf16[16,32,256]{2,1,0:T(8,128)(2,1)S(1)}, u32[]{:S(2)}, u32[]{:S(2)}) async-start(bf16[16,32,256]{2,1,0:T(8,128)(2,1)} %bitcast.73), calls=%async_computation.7 | async-start | bytes 524288 | tf_op jit(solution)/shard_map/all_to_all | solution.py:48
  278.9 0.7 reshape.97
  279.6 7.1 %all-to-all-done.7 = bf16[16,32,256]{2,1,0:T(8,128)(2,1)S(1)} async-done(((bf16[16,32,256]{2,1,0:T(8,128)(2,1)}), bf16[16,32,256]{2,1,0:T(8,128)(2,1)S(1)}, u32[]{:S(2)}, u32[]{:S(2)}) %all-to-all-start.7) | async-done | bytes 262176 | tf_op jit(solution)/shard_map/all_to_all | solution.py:48
  286.7 8.2 %all-to-all-start.6 = ((bf16[32,4,256]{2,1,0:T(4,128)(2,1)}), bf16[32,4,256]{2,1,0:T(4,128)(2,1)S(1)}, u32[]{:S(2)}, u32[]{:S(2)}) async-start(bf16[32,4,256]{2,1,0:T(4,128)(2,1)} %reshape.97), calls=%async_computation.6 | async-start | bytes 131072 | tf_op jit(solution)/shard_map/all_to_all | solution.py:194
  295.0 12.9 %all-to-all-done.6 = bf16[32,4,256]{2,1,0:T(4,128)(2,1)S(1)} async-done(((bf16[32,4,256]{2,1,0:T(4,128)(2,1)}), bf16[32,4,256]{2,1,0:T(4,128)(2,1)S(1)}, u32[]{:S(2)}, u32[]{:S(2)}) %all-to-all-start.6) | async-done | bytes 65568 | tf_op jit(solution)/shard_map/all_to_all | solution.py:194
  308.1 0.7 broadcast_in_dim.69
  308.9 3.5 %all-to-all-start.8 = ((bf16[16,32,256]{2,1,0:T(8,128)(2,1)}), bf16[16,32,256]{2,1,0:T(8,128)(2,1)S(1)}, u32[]{:S(2)}, u32[]{:S(2)}) async-start(bf16[16,32,256]{2,1,0:T(8,128)(2,1)} %broadcast_in_dim.69), calls=%async_computation.8 | async-start | bytes 524288 | tf_op jit(solution)/shard_map/all_to_all | solution.py:26
  312.4 0.6 fusion.57
  313.1 6.9 %all-to-all-done.8 = bf16[16,32,256]{2,1,0:T(8,128)(2,1)S(1)} async-done(((bf16[16,32,256]{2,1,0:T(8,128)(2,1)}), bf16[16,32,256]{2,1,0:T(8,128)(2,1)S(1)}, u32[]{:S(2)}, u32[]{:S(2)}) %all-to-all-start.8) | async-done | bytes 262176 | tf_op jit(solution)/shard_map/all_to_all | solution.py:26
  320.0 0.7 copy.109
  (80 shorter events, 4.0 us)
Async XLA Ops:
  7.2 236.4 %copy-start = (bf16[1,128,4096]{2,1,0:T(8,128)(2,1)S(1)}, bf16[1,128,4096]{2,1,0:T(8,128)(2,1)}, u32[]{:S(2)}) copy-start(bf16[1,128,4096]{2,1,0:T(8,128)(2,1)} %param.37) | copy-start | bytes 3145732
  7.2 19.6 %copy-start.7 = (bf16[128,128]{1,0:T(8,128)(2,1)S(1)}, bf16[128,128]{1,0:T(8,128)(2,1)}, u32[]{:S(2)}) copy-start(bf16[128,128]{1,0:T(8,128)(2,1)} %param.40) | copy-start | bytes 98308
  7.2 121.3 %all-gather.6.cloned.1.call-start = ((), (), s32[]{:S(2)}) async-start(), calls=%async_computation.9 | async-start | bytes 4325376 | tf_op jit(solution)/shard_map/all_gather | solution.py:21
  8.9 100.2 %copy-start.12 = (s32[32,2]{0,1:T(2,128)S(1)}, s32[32,2]{0,1:T(2,128)}, u32[]{:S(2)}) copy-start(s32[32,2]{0,1:T(2,128)} %param.34) | copy-start | bytes 772
  8.9 100.8 %copy-start.1 = (bf16[32,4096]{1,0:T(8,128)(2,1)S(1)}, bf16[32,4096]{1,0:T(8,128)(2,1)}, u32[]{:S(2)}) copy-start(bf16[32,4096]{1,0:T(8,128)(2,1)} %param.21) | copy-start | bytes 786436
  8.9 101.0 %copy-start.18 = (f32[256]{0:T(256)S(1)}, f32[256]{0:T(256)}, u32[]{:S(2)}) copy-start(f32[256]{0:T(256)} %param.30) | copy-start | bytes 3076
  11.0 99.5 %all-to-all-start = ((bf16[16,256,128]{2,1,0:T(8,128)(2,1)}), bf16[16,256,128]{2,1,0:T(8,128)(2,1)S(1)}, u32[]{:S(2)}, u32[]{:S(2)}) async-start(bf16[16,256,128]{2,1,0:T(8,128)(2,1)} %broadcast_in_dim.59), calls=%async_computation | async-start | bytes 2097152 | tf_op jit(solution)/shard_map/all_to_all | solution.py:26
  26.7 223.7 %all-gather.10.cloned.1.call-start = ((), (), s32[]{:S(2)}) async-start(), calls=%async_computation.11 | async-start | bytes 1572864 | tf_op jit(solution)/shard_map/all_gather | solution.py:74
  109.9 18.6 %copy-start.19 = (f32[32]{0:T(128)}, f32[32]{0:T(128)S(1)}, u32[]{:S(2)}) copy-start(f32[32]{0:T(128)S(1)} %add_rsqrt_fusion.1) | copy-start | bytes 388
  125.1 3.4 %copy-start.11 = (f32[4096]{0:T(1024)S(1)}, f32[4096]{0:T(1024)}, u32[]{:S(2)}) copy-start(f32[4096]{0:T(1024)} %param.24) | copy-start | bytes 49156
  128.4 2.2 copy-start.4
  128.4 2.2 copy-start.17
  130.7 0.6 copy-start.8
  135.7 4.0 %copy-start.5 = (f32[32,256]{1,0:T(8,128)}, f32[32,256]{1,0:T(8,128)S(1)}, u32[]{:S(2)}) copy-start(f32[32,256]{1,0:T(8,128)S(1)} %multiply_add_fusion) | copy-start | bytes 98308
  135.8 12.7 %copy-start.16 = (s32[64]{0:T(128)S(1)}, s32[64]{0:T(128)}, u32[]{:S(2)}) copy-start(s32[64]{0:T(128)} %eq.54) | copy-start | bytes 772
  139.7 21.5 %copy-start.13 = (s32[32,2]{0,1:T(2,128)S(1)}, s32[32,2]{0,1:T(2,128)}, u32[]{:S(2)}) copy-start(s32[32,2]{0,1:T(2,128)} %param.34) | copy-start | bytes 772
  139.7 29.3 %copy-start.6 = (f32[4096]{0:T(1024)S(1)}, f32[4096]{0:T(1024)}, u32[]{:S(2)}) copy-start(f32[4096]{0:T(1024)} %param.32) | copy-start | bytes 49156
  141.6 15.0 %all-to-all-start.2 = ((bf16[16,2,4096]{2,1,0:T(2,128)(2,1)}), bf16[16,2,4096]{2,1,0:T(2,128)(2,1)S(1)}, u32[]{:S(2)}, u32[]{:S(2)}) async-start(bf16[16,2,4096]{2,1,0:T(2,128)(2,1)} %reshape.93), calls=%async_computation.2 | async-start | bytes 524288 | tf_op jit(solution)/shard_map/all_to_all | solution.py:48
  157.7 11.0 %all-to-all-start.3 = ((bf16[16,2,4096]{2,1,0:T(2,128)(2,1)}), bf16[16,2,4096]{2,1,0:T(2,128)(2,1)S(1)}, u32[]{:S(2)}, u32[]{:S(2)}) async-start(bf16[16,2,4096]{2,1,0:T(2,128)(2,1)} %broadcast_in_dim.61), calls=%async_computation.3 | async-start | bytes 524288 | tf_op jit(solution)/shard_map/all_to_all | solution.py:26
  169.0 1.8 copy-start.2
  169.5 12.8 %copy-start.9 = (bf16[128,128]{1,0:T(8,128)(2,1)S(1)}, bf16[128,128]{1,0:T(8,128)(2,1)}, u32[]{:S(2)}) copy-start(bf16[128,128]{1,0:T(8,128)(2,1)} %param.39) | copy-start | bytes 98308
  169.5 12.8 %copy-start.10 = (bf16[128,128]{1,0:T(8,128)(2,1)S(1)}, bf16[128,128]{1,0:T(8,128)(2,1)}, u32[]{:S(2)}) copy-start(bf16[128,128]{1,0:T(8,128)(2,1)} %param.38) | copy-start | bytes 98308
  170.8 70.9 %all-to-all-start.4 = ((bf16[32,4,4096]{2,1,0:T(4,128)(2,1)}), bf16[32,4,4096]{2,1,0:T(4,128)(2,1)S(1)}, u32[]{:S(2)}, u32[]{:S(2)}) async-start(bf16[32,4,4096]{2,1,0:T(4,128)(2,1)} %reshape.94), calls=%async_computation.4 | async-start | bytes 2097152 | tf_op jit(solution)/shard_map/all_to_all | solution.py:186
  182.3 82.1 %all-gather.8.cloned.1.call-start = ((), (), s32[]{:S(2)}) async-start(), calls=%async_computation.10 | async-start | bytes 2162688 | tf_op jit(solution)/shard_map/all_gather | solution.py:21
  245.6 4.8 %copy-start.15 = (bf16[4096]{0:T(1024)(128)(2,1)S(1)}, bf16[4096]{0:T(1024)(128)(2,1)}, u32[]{:S(2)}) copy-start(bf16[4096]{0:T(1024)(128)(2,1)} %param.41) | copy-start | bytes 24580
  246.7 25.0 %all-to-all-start.5 = ((bf16[16,128,256]{2,1,0:T(8,128)(2,1)}), bf16[16,128,256]{2,1,0:T(8,128)(2,1)S(1)}, u32[]{:S(2)}, u32[]{:S(2)}) async-start(bf16[16,128,256]{2,1,0:T(8,128)(2,1)} %bitcast.71), calls=%async_computation.5 | async-start | bytes 2097152 | tf_op jit(solution)/shard_map/all_to_all | solution.py:48
  250.5 13.9 %copy-start.3 = (bf16[32,4096]{1,0:T(8,128)(2,1)S(1)}, bf16[32,4096]{1,0:T(8,128)(2,1)}, u32[]{:S(2)}) copy-start(bf16[32,4096]{1,0:T(8,128)(2,1)} %copy-done.2) | copy-start | bytes 786436
  265.9 5.6 %copy-start.14 = (s32[32,2]{0,1:T(2,128)S(1)}, s32[32,2]{0,1:T(2,128)}, u32[]{:S(2)}) copy-start(s32[32,2]{0,1:T(2,128)} %param.34) | copy-start | bytes 772
  271.7 15.0 %all-to-all-start.7 = ((bf16[16,32,256]{2,1,0:T(8,128)(2,1)}), bf16[16,32,256]{2,1,0:T(8,128)(2,1)S(1)}, u32[]{:S(2)}, u32[]{:S(2)}) async-start(bf16[16,32,256]{2,1,0:T(8,128)(2,1)} %bitcast.73), calls=%async_computation.7 | async-start | bytes 524288 | tf_op jit(solution)/shard_map/all_to_all | solution.py:48
  286.7 21.2 %all-to-all-start.6 = ((bf16[32,4,256]{2,1,0:T(4,128)(2,1)}), bf16[32,4,256]{2,1,0:T(4,128)(2,1)S(1)}, u32[]{:S(2)}, u32[]{:S(2)}) async-start(bf16[32,4,256]{2,1,0:T(4,128)(2,1)} %reshape.97), calls=%async_computation.6 | async-start | bytes 131072 | tf_op jit(solution)/shard_map/all_to_all | solution.py:194
  308.9 11.1 %all-to-all-start.8 = ((bf16[16,32,256]{2,1,0:T(8,128)(2,1)}), bf16[16,32,256]{2,1,0:T(8,128)(2,1)S(1)}, u32[]{:S(2)}, u32[]{:S(2)}) async-start(bf16[16,32,256]{2,1,0:T(8,128)(2,1)} %broadcast_in_dim.69), calls=%async_computation.8 | async-start | bytes 524288 | tf_op jit(solution)/shard_map/all_to_all | solution.py:26
Sparse Core Ops, SparseCore 0:
  10.7 107.2 all-gather.5
  120.0 17.3 all-gather.9
  185.2 79.0 all-gather.7
where the time goes:
time: 329 us; the launch traced here: 327 us
  waiting for transfers between devices  111 us (34%)
  blocking collectives  95 us (29%)
  starting transfers between devices  59.9 us (18%)
  local copies, waits for them, and re-layouts  23.7 us (7%)
  matrix products  18.1 us (6%)
  between operations  14.3 us (4%)
  other arithmetic  5.56 us (2%)
    all_gather x1, blocking collectives, all_blocks(): pieces = lax.all_gather(pieces, axes[k])  82.2 us
    all_to_all x1, waiting for transfers between devices, on_device(): lax.all_to_all(outgoing, EP, split_axis=0, concat_axis=0, tiled=True)  58.6 us
    all_to_all x3, starting transfers between devices, copy_for_each(): return lax.all_to_all(copies, axis, split_axis=0, concat_axis=0, tiled=True)  22.8 us
    all_to_all x3, starting transfers between devices, summed_on_arrival(): lax.all_to_all(pieces, axis, split_axis=0, concat_axis=0, tiled=True)  17.2 us
    all_to_all x3, waiting for transfers between devices, summed_on_arrival(): lax.all_to_all(pieces, axis, split_axis=0, concat_axis=0, tiled=True)  14.7 us
    all_to_all x3, waiting for transfers between devices, copy_for_each(): return lax.all_to_all(copies, axis, split_axis=0, concat_axis=0, tiled=True)  14.4 us
    all_to_all x1, waiting for transfers between devices, on_device(): lax.all_to_all(total.reshape(sources, items, total.shape[1]), EP, split_a...  12.9 us
    all_to_all x1, blocking collectives, copy_for_each(): return lax.all_to_all(copies, axis, split_axis=0, concat_axis=0, tiled=True)  12.7 us
  transfers between devices with their start and end apart: 11, of which 7 were waited for; matrix products, arithmetic and copies ran while one was open for 13% of the time, Pallas kernels for 0%

commit v1 on v0

v1 whole, which is shorter than its diff:
```python
import jax
import jax.numpy as jnp
from jax import lax
from jax.sharding import Mesh
from jax.sharding import PartitionSpec as P

TOP_K = 2
EP = ("ep_0", "ep_1")


epsilon = 1e-06
decay_scale = 8.0


def exchange(pieces, axis):
    return lax.all_to_all(pieces, axis, split_axis=0, concat_axis=0, tiled=True)


def copies_to_all(value, axis):
    return exchange(jnp.broadcast_to(value, (lax.axis_size(axis), *value.shape)), axis)


def features_cut(rows, devices):
    count, width = rows.shape
    return rows.reshape(count, devices, width // devices).swapaxes(0, 1)


def features_joined(pieces):
    devices, count, share = pieces.shape
    return pieces.swapaxes(0, 1).reshape(count, devices * share)


def rms_scale(rows, gain):
    values = rows.astype(jnp.float32)
    inverse = lax.rsqrt(jnp.mean(values * values, axis=-1, keepdims=True) + epsilon)
    return (values * inverse * gain).astype(jnp.bfloat16)


def dot(left, right):
    return jnp.dot(left, right, preferred_element_type=jnp.float32)


def lane_blocks(weight, lanes):
    return [weight[:, at : at + lanes] for at in range(0, weight.shape[1], lanes)]


def on_device(
    tokens,
    recur_state,
    conv_state,
    mix_gain,
    in_weight,
    gate_weight,
    conv_taps,
    recur_gate_blocks,
    input_gate_blocks,
    decay_rate,
    out_weight,
    ffn_gain,
    router_weight,
    routes,
    expert_gate,
    expert_up,
    expert_down,
    dense_gate,
    dense_up,
    dense_down,
    branch_gate,
):
    batch_rows, width = tokens.shape
    depth, channels = in_weight.shape
    lanes = out_weight.shape[1]
    columns = lax.axis_size("tp")
    share = width // columns
    parts = [*lane_blocks(in_weight, lanes), *lane_blocks(gate_weight, lanes), out_weight, dense_gate, dense_up, dense_down]
    whole = lax.all_gather(jnp.concatenate(parts, axis=0), EP)
    pieces, at = [], 0
    for part in parts:
        pieces.append(whole[:, at : at + part.shape[0]])
        at += part.shape[0]
    per = channels // lanes
    by_rows = lambda piece: piece.reshape(-1, lanes)
    by_columns = lambda piece: piece.swapaxes(0, 1).reshape(piece.shape[1], -1)
    in_whole = jnp.concatenate([by_rows(p) for p in pieces[:per]], axis=1)
    gate_whole = jnp.concatenate([by_rows(p) for p in pieces[per : 2 * per]], axis=1)
    out_piece, dense_gate_piece, dense_up_piece, dense_down_piece = pieces[2 * per :]

    normed = rms_scale(tokens, mix_gain)
    x_branch = dot(normed, in_whole).astype(jnp.bfloat16)
    gate_branch = dot(normed, gate_whole).astype(jnp.bfloat16)
    window = jnp.concatenate([conv_state, x_branch[:, None, :]], axis=1)
    conv_out = jnp.sum(window.astype(jnp.float32) * conv_taps[None], axis=1).astype(jnp.bfloat16)
    new_conv_state = window[:, 1:, :]
    blocks = conv_out.reshape(batch_rows, recur_gate_blocks.shape[0], recur_gate_blocks.shape[1])

    def block_gate(maps):
        sums = jnp.einsum("bhi,hij->bhj", blocks, maps, preferred_element_type=jnp.float32)
        return jax.nn.sigmoid(sums.reshape(batch_rows, channels))

    recur_gate = block_gate(recur_gate_blocks)
    input_gate = block_gate(input_gate_blocks)
    log_decay = -decay_scale * recur_gate * decay_rate
    new_state = jnp.exp(log_decay) * recur_state + jnp.sqrt(
        -jnp.expm1(2.0 * log_decay)
    ) * input_gate * conv_out.astype(jnp.float32)
    mixer_rows = (new_state * jax.nn.gelu(gate_branch.astype(jnp.float32))).astype(jnp.bfloat16)
    mixer_part = dot(mixer_rows, by_columns(out_piece)).astype(jnp.bfloat16)

    mixed_share = exchange(features_cut(mixer_part, columns), "tp").astype(jnp.float32).sum(axis=0)
    own_tokens = lax.dynamic_slice_in_dim(tokens, lax.axis_index("tp") * share, share, 1)
    resid_share = (own_tokens.astype(jnp.float32) + mixed_share).astype(jnp.bfloat16)

    experts = router_weight.shape[1]
    capacity = 2 * batch_rows * TOP_K // experts
    flat_ids = routes.reshape(batch_rows * TOP_K)
    onehot = (
        flat_ids[:, None] == lax.broadcasted_iota(jnp.int32, (batch_rows * TOP_K, experts), 1)
    ).astype(jnp.int32)
    rank = jnp.sum((jnp.cumsum(onehot, axis=0) - onehot) * onehot, axis=1)
    slot_of = (flat_ids * capacity + rank).reshape(batch_rows, TOP_K)
    slot_rows = lax.broadcasted_iota(jnp.int32, (experts * capacity, batch_rows), 0)
    slot_cols = lax.broadcasted_iota(jnp.int32, (batch_rows, experts * capacity), 1)
    dispatch = jnp.zeros((experts * capacity, batch_rows), jnp.bfloat16)
    for pick in range(TOP_K):
        dispatch = dispatch + (slot_rows == slot_of[None, :, pick]).astype(jnp.bfloat16)

    outgoing = dot(dispatch, resid_share).astype(jnp.bfloat16).reshape(experts, capacity, share)
    arrived = exchange(outgoing, EP)
    sources, items, _ = arrived.shape
    slots = sources * items
    both = jnp.concatenate([arrived.reshape(slots, share), resid_share], axis=0)
    all_rows = features_joined(copies_to_all(both, "tp"))
    all_normed = rms_scale(all_rows, ffn_gain)
    rows, normed_ffn = all_normed[:slots], all_normed[slots:]

    act = (jax.nn.silu(dot(rows, expert_gate[0])) * dot(rows, expert_up[0])).astype(jnp.bfloat16)
    expert_part = dot(act, expert_down[0]).astype(jnp.bfloat16)
    dense_first = dot(normed_ffn, by_rows(dense_gate_piece))
    dense_second = dot(normed_ffn, by_rows(dense_up_piece))
    dense_act = (jax.nn.silu(dense_first) * dense_second).astype(jnp.bfloat16)
    dense_part = dot(dense_act, by_columns(dense_down_piece)).astype(jnp.bfloat16)
    parts_cut = features_cut(jnp.concatenate([expert_part, dense_part], axis=0), columns)
    sums = exchange(parts_cut, "tp").astype(jnp.float32).sum(axis=0)
    total, dense_share = sums[:slots].astype(jnp.bfloat16), sums[slots:]

    router_logits = dot(normed_ffn, router_weight)
    expert_ids = lax.broadcasted_iota(jnp.int32, (batch_rows, TOP_K, experts), 2)
    picked = jnp.sum(
        jnp.where(routes[:, :, None] == expert_ids, router_logits[:, None, :], 0.0), axis=2
    )
    route_weight = jax.nn.sigmoid(picked - picked[:, ::-1]).astype(jnp.bfloat16)
    combine = jnp.zeros((batch_rows, experts * capacity), jnp.bfloat16)
    for pick in range(TOP_K):
        combine = combine + jnp.where(
            slot_cols == slot_of[:, pick : pick + 1],
            route_weight[:, pick : pick + 1],
            jnp.zeros((), jnp.bfloat16),
        )
    branch_weight = jax.nn.sigmoid(dot(normed_ffn, branch_gate))

    returned = exchange(total.reshape(sources, items, share), EP)
    moe = dot(combine, returned.reshape(experts * capacity, share))
    out_share = (
        resid_share.astype(jnp.float32) + moe + branch_weight[:, None] * dense_share
    ).astype(jnp.bfloat16)
    layer_out = features_joined(copies_to_all(out_share, "tp"))
    return (layer_out, new_state, new_conv_state)


def solution(mesh):
    split = Mesh(mesh.devices.reshape(16, 2, mesh.shape["tp"]), ("ep_0", "ep_1", "tp"))
    in_specs = (
        P(EP, None),
        P(EP, "tp"),
        P(EP, None, "tp"),
        P(),
        P(EP, "tp"),
        P(EP, "tp"),
        P(None, "tp"),
        P("tp", None, None),
        P("tp", None, None),
        P("tp"),
        P("tp", EP),
        P(),
        P(),
        P(EP, None),
        P(EP, None, "tp"),
        P(EP, None, "tp"),
        P(EP, "tp", None),
        P(EP, "tp"),
        P(EP, "tp"),
        P("tp", EP),
        P(),
    )
    out_specs = (P(EP, None), P(EP, "tp"), P(EP, None, "tp"))
    return jax.shard_map(
        on_device, mesh=split, in_specs=in_specs, out_specs=out_specs, check_vma=False
    )
```

time: 329 us -> 264 us (0.80)
  blocking collectives: 95 us -> 21 us
  waiting for transfers between devices: 111 us -> 143 us
  starting transfers between devices: 59.9 us -> 30.3 us
  local copies, waits for them, and re-layouts: 23.7 us -> 30.5 us
  matrix products: 18.1 us -> 14.1 us
    all_gather x1 -> x0, blocking collectives: 82.2 us -> none  [all_blocks(): pieces = lax.all_gather(pieces, axes[k])]
    all_gather x3 -> x1, waiting for transfers between devices: 9.95 us -> 81.4 us  [on_device(): whole = lax.all_gather(jnp.concatenate(parts, axis=0), EP)]
    all_to_all x8 -> x5, waiting for transfers between devices: 101 us -> 61.6 us  [exchange(): return lax.all_to_all(pieces, axis, split_axis=0, concat_axis=0, tiled=True)]
    all_to_all x8 -> x5, starting transfers between devices: 59.8 us -> 30.3 us  [exchange(): return lax.all_to_all(pieces, axis, split_axis=0, concat_axis=0, tiled=True)]
    all_to_all x1, blocking collectives: 12.7 us -> 21 us  [exchange(): return lax.all_to_all(pieces, axis, split_axis=0, concat_axis=0, tiled=True)]
    unnamed x42 -> x57, local copies, waits for them, and re-layouts: 0.83 us -> 9.01 us
    slice x0 -> x2, local copies, waits for them, and re-layouts: none -> 6.68 us  [the longest x1 6.67 us: on_device(): pieces.append(whole[:, at:at + part.shape[0]])]
    reshape x8 -> x7, local copies, waits for them, and re-layouts: 7.47 us -> 3.38 us  [the longest x2 1.95 us: features_cut(): return rows.reshape(count, devices, width // devices).swapaxes(0, 1)]
  transfers between devices with their start and end apart: 11 -> 6, of which waited for: 7 -> 6; matrix products, arithmetic and copies ran while one was open for 13% -> 3% of each run, Pallas kernels for 0% -> 0%
where the time goes in v1:
time: 264 us; the launch traced here: 262 us
  waiting for transfers between devices  143 us (54%)
  local copies, waits for them, and re-layouts  30.5 us (12%)
  starting transfers between devices  30.3 us (11%)
  blocking collectives  21 us (8%)
  between operations  14.5 us (5%)
  matrix products  14.1 us (5%)
  other arithmetic  8.27 us (3%)
    all_gather x1, waiting for transfers between devices, on_device(): whole = lax.all_gather(jnp.concatenate(parts, axis=0), EP)  81.4 us
    all_to_all x5, waiting for transfers between devices, exchange(): return lax.all_to_all(pieces, axis, split_axis=0, concat_axis=0, tiled=True)  61.6 us
    all_to_all x5, starting transfers between devices, exchange(): return lax.all_to_all(pieces, axis, split_axis=0, concat_axis=0, tiled=True)  30.3 us
    all_to_all x1, blocking collectives, exchange(): return lax.all_to_all(pieces, axis, split_axis=0, concat_axis=0, tiled=True)  21 us
    dot_general x10, matrix products, dot(): return jnp.dot(left, right, preferred_element_type=jnp.float32)  12.1 us
    unnamed x57, local copies, waits for them, and re-layouts  9.01 us
    slice x1, local copies, waits for them, and re-layouts, on_device(): pieces.append(whole[:, at:at + part.shape[0]])  6.67 us
    transpose x3, local copies, waits for them, and re-layouts, on_device(): by_columns = lambda piece: piece.swapaxes(0, 1).reshape(piece.shape[1], -1)  6 us
  transfers between devices with their start and end apart: 6, of which 6 were waited for; matrix products, arithmetic and copies ran while one was open for 3% of the time, Pallas kernels for 0%

profile of v1, /device:TPU:1, one launch (start us, length us, event | category | flops | bytes accessed | tf_op | source)
XLA Modules:
  0.0 261.8 jit_solution(17885081153248645924)
XLA Ops:
  7.2 0.8 slice_dynamic-update-slice_fusion.3
  8.1 0.8 slice_dynamic-update-slice_fusion.2
  8.8 0.8 slice_dynamic-update-slice_fusion.1
  9.6 0.8 slice_dynamic-update-slice_fusion
  10.4 0.9 constant_dynamic-update-slice_fusion.3
  11.2 0.8 constant_dynamic-update-slice_fusion.2
  12.0 0.8 constant_dynamic-update-slice_fusion.1
  12.8 0.8 constant_dynamic-update-slice_fusion
  13.5 0.7 copy-done.4
  14.3 0.8 copy.94
  16.2 1.1 fusion.45
  17.3 1.2 broadcast_multiply_fusion
  18.6 81.4 %all-gather.3.cloned.1.call-done = bf16[36864,128]{1,0:T(8,128)(2,1)} async-done(((bf16[1152,128]{1,0:T(8,128)(2,1)}), bf16[36864,128]{1,0:T(8,128)(2,1)}) %all-gather.3.cloned.1.call-update) | async-done | bytes 9437200 | tf_op jit(solution)/shard_map/all_gather | solution.py:76
  99.9 6.7 %fusion.130 = (bf16[32,128,128]{2,1,0:T(8,128)(2,1)}, bf16[128,32,128]{2,0,1:T(8,128)(2,1)}, bf16[32,128,128]{2,1,0:T(8,128)(2,1)}, bf16[32,128,128]{2,1,0:T(8,1...) fusion(bf16[32,1152,128]{2,1,0:T(8,128)(2,1)} %bitcast.79), kind=kLoop, calls=%fused_computation.153 | loop fusion | bytes 14680064 | tf_op jit(solution)/shard_map/slice | solution.py:79
  106.6 1.8 slice_bitcast_fusion
  109.3 0.6 copy-done.9
  109.9 1.0 fusion.16
  111.0 0.7 div.41
  111.7 1.0 fusion.12
  112.8 0.7 div.43
  113.5 2.9 %copy.92 = bf16[256,32,128]{0,2,1:T(8,128)(2,1)} copy(bf16[256,32,128]{2,0,1:T(8,128)(2,1)S(1)} %slice_bitcast_fusion) | data formatting | bytes 4194304 | tf_op jit(solution)/shard_map/transpose | solution.py:83
  116.4 0.8 multiply_add_fusion
  117.2 3.8 %convolution_convert_fusion.2 = bf16[32,4096]{1,0:T(8,128)(2,1)S(1)} fusion(bf16[256,4096]{0,1:T(8,128)(2,1)} %bitcast.86, f32[32,256]{1,0:T(8,128)S(1)} %multiply_add_fusion, bf16[4096,128]{1,0:T(8,128)(2,1)} %bitcast.87, bf16[4096,128]{1,0:T(8,128)(2,1)} %bitcast.88, bf16[32,4096]{1,0:T(8,128)(2,1)S(1)} %copy-done.5, f32[4096]{0:T(1024)} %param.24, ...), kind=kOutput, calls=%fused_computation.2 | convolution fusion | flops 139165696 | bytes 4767872 | tf_op jit(solution)/shard_map/dot_general | solution.py:40
  121.1 0.7 copy.111
  121.8 6.5 %all-to-all-start = ((bf16[16,32,256]{2,1,0:T(8,128)(2,1)}), bf16[16,32,256]{2,1,0:T(8,128)(2,1)S(1)}, u32[]{:S(2)}, u32[]{:S(2)}) async-start(bf16[16,32,256]{2,1,0:T(8,128)(2,1)} %bitcast.77), calls=%async_computation | async-start | bytes 524288 | tf_op jit(solution)/shard_map/all_to_all | solution.py:16
  128.4 8.1 %all-to-all-done = bf16[16,32,256]{2,1,0:T(8,128)(2,1)S(1)} async-done(((bf16[16,32,256]{2,1,0:T(8,128)(2,1)}), bf16[16,32,256]{2,1,0:T(8,128)(2,1)S(1)}, u32[]{:S(2)}, u32[]{:S(2)}) %all-to-all-start) | async-done | bytes 262176 | tf_op jit(solution)/shard_map/all_to_all | solution.py:16
  136.8 21.0 %all_to_all.30 = bf16[32,4,256]{2,1,0:T(4,128)(2,1)S(1)} all-to-all(bf16[32,4,256]{2,1,0:T(4,128)(2,1)S(1)} %reshape.106), channel_id=1, replica_groups=mesh['ep_0'=16,'ep_1'=2,'tp'=16] {'ep_0','ep_1'}, dimensions={0} | all-to-all | bytes 131072 | tf_op jit(solution)/shard_map/all_to_all | solution.py:16
  157.9 1.2 broadcast_in_dim.53
  159.1 3.7 %all-to-all-start.2 = ((bf16[16,160,256]{2,1,0:T(8,128)(2,1)}), bf16[16,160,256]{2,1,0:T(8,128)(2,1)S(1)}, u32[]{:S(2)}, u32[]{:S(2)}) async-start(bf16[16,160,256]{2,1,0:T(8,128)(2,1)} %broadcast_in_dim.53), calls=%async_computation.2 | async-start | bytes 2621440 | tf_op jit(solution)/shard_map/all_to_all | solution.py:16
  162.8 1.3 copy.97
  164.1 16.8 %all-to-all-done.2 = bf16[16,160,256]{2,1,0:T(8,128)(2,1)S(1)} async-done(((bf16[16,160,256]{2,1,0:T(8,128)(2,1)}), bf16[16,160,256]{2,1,0:T(8,128)(2,1)S(1)}, u32[]{:S(2)}, u32[]{:S(2)}) %all-to-all-start.2) | async-done | bytes 1310752 | tf_op jit(solution)/shard_map/all_to_all | solution.py:16
  182.3 0.8 copy-done.20
  183.1 1.1 fusion.40
  184.7 3.1 %convolution_convert_fusion = bf16[128,4096]{1,0:T(8,128)(2,1)} fusion(bf16[1,128,4096]{2,1,0:T(8,128)(2,1)S(1)} %copy-done, bf16[1,4096,128]{2,1,0:T(8,128)(2,1)} %param.36, bf16[160,4096]{1,0:T(8,128)(2,1)S(1)} %multiply_convert_fusion, f32[128,128]{1,0:T(8,128)} %fusion.40), kind=kOutput, calls=%fused_computation | convolution fusion | flops 269058048 | bytes 4259840 | tf_op jit(solution)/shard_map/dot_general | solution.py:40
  187.8 2.6 %convolution_convert_fusion.1 = bf16[32,4096]{1,0:T(8,128)(2,1)} fusion(bf16[128,4096]{0,1:T(8,128)(2,1)} %bitcast.85, bf16[4096,128]{1,0:T(8,128)(2,1)S(1)} %bitcast.83, bf16[160,4096]{1,0:T(8,128)(2,1)S(1)} %multiply_convert_fusion, f32[32,128]{1,0:T(8,128)S(1)} %fusion.51), kind=kOutput, calls=%fused_computation.1 | convolution fusion | flops 67264512 | bytes 2637824 | tf_op jit(solution)/shard_map/dot_general | solution.py:40
  190.4 1.4 pad_maximum_fusion
  191.8 1.2 copy.110
  193.1 4.6 %all-to-all-start.3 = ((bf16[16,160,256]{2,1,0:T(8,128)(2,1)}), bf16[16,160,256]{2,1,0:T(8,128)(2,1)}, u32[]{:S(2)}, u32[]{:S(2)}) async-start(bf16[16,160,256]{2,1,0:T(8,128)(2,1)} %bitcast.81), calls=%async_computation.3 | async-start | bytes 2621440 | tf_op jit(solution)/shard_map/all_to_all | solution.py:16
  198.2 16.9 %all-to-all-done.3 = bf16[16,160,256]{2,1,0:T(8,128)(2,1)} async-done(((bf16[16,160,256]{2,1,0:T(8,128)(2,1)}), bf16[16,160,256]{2,1,0:T(8,128)(2,1)}, u32[]{:S(2)}, u32[]{:S(2)}) %all-to-all-start.3) | async-done | bytes 1310752 | tf_op jit(solution)/shard_map/all_to_all | solution.py:16
  215.1 1.5 convert_reduce_fusion
  216.6 0.7 reshape.112
  217.2 11.9 %all-to-all-start.4 = ((bf16[32,4,256]{2,1,0:T(4,128)(2,1)}), bf16[32,4,256]{2,1,0:T(4,128)(2,1)S(1)}, u32[]{:S(2)}, u32[]{:S(2)}) async-start(bf16[32,4,256]{2,1,0:T(4,128)(2,1)} %reshape.112), calls=%async_computation.4 | async-start | bytes 131072 | tf_op jit(solution)/shard_map/all_to_all | solution.py:16
  229.4 12.8 %all-to-all-done.4 = bf16[32,4,256]{2,1,0:T(4,128)(2,1)S(1)} async-done(((bf16[32,4,256]{2,1,0:T(4,128)(2,1)}), bf16[32,4,256]{2,1,0:T(4,128)(2,1)S(1)}, u32[]{:S(2)}, u32[]{:S(2)}) %all-to-all-start.4) | async-done | bytes 65568 | tf_op jit(solution)/shard_map/all_to_all | solution.py:16
  242.4 0.7 broadcast_in_dim.61
  243.2 3.5 %all-to-all-start.5 = ((bf16[16,32,256]{2,1,0:T(8,128)(2,1)}), bf16[16,32,256]{2,1,0:T(8,128)(2,1)S(1)}, u32[]{:S(2)}, u32[]{:S(2)}) async-start(bf16[16,32,256]{2,1,0:T(8,128)(2,1)} %broadcast_in_dim.61), calls=%async_computation.5 | async-start | bytes 524288 | tf_op jit(solution)/shard_map/all_to_all | solution.py:16
  246.7 0.6 fusion.64
  247.3 6.9 %all-to-all-done.5 = bf16[16,32,256]{2,1,0:T(8,128)(2,1)S(1)} async-done(((bf16[16,32,256]{2,1,0:T(8,128)(2,1)}), bf16[16,32,256]{2,1,0:T(8,128)(2,1)S(1)}, u32[]{:S(2)}, u32[]{:S(2)}) %all-to-all-start.5) | async-done | bytes 262176 | tf_op jit(solution)/shard_map/all_to_all | solution.py:16
  254.2 0.7 copy.103
  (83 shorter events, 5.1 us)
Async XLA Ops:
  7.2 177.5 %copy-start = (bf16[1,128,4096]{2,1,0:T(8,128)(2,1)S(1)}, bf16[1,128,4096]{2,1,0:T(8,128)(2,1)}, u32[]{:S(2)}) copy-start(bf16[1,128,4096]{2,1,0:T(8,128)(2,1)} %param.37) | copy-start | bytes 3145732
  7.2 92.8 %all-gather.3.cloned.1.call-start = ((), (), s32[]{:S(2)}) async-start(), calls=%async_computation.6 | async-start | bytes 9732096 | tf_op jit(solution)/shard_map/all_gather | solution.py:76
  13.5 0.7 copy-start.4
  17.3 91.1 %copy-start.23 = (f32[32]{0:T(128)}, f32[32]{0:T(128)S(1)}, u32[]{:S(2)}) copy-start(f32[32]{0:T(128)S(1)} %add_rsqrt_fusion.1) | copy-start | bytes 388
  106.6 1.8 copy-start.5
  106.6 1.8 copy-start.22
  108.4 0.8 copy-start.6
  108.4 0.8 copy-start.15
  109.3 0.6 copy-start.9
  113.5 2.9 %copy-start.7 = (f32[32,256]{1,0:T(8,128)S(1)}, f32[32,256]{1,0:T(8,128)}, u32[]{:S(2)}) copy-start(f32[32,256]{1,0:T(8,128)} %div.41) | copy-start | bytes 98308
  113.5 2.9 %copy-start.8 = (f32[32,256]{1,0:T(8,128)S(1)}, f32[32,256]{1,0:T(8,128)}, u32[]{:S(2)}) copy-start(f32[32,256]{1,0:T(8,128)} %div.43) | copy-start | bytes 98308
  117.2 3.9 %copy-start.10 = (f32[32,256]{1,0:T(8,128)}, f32[32,256]{1,0:T(8,128)S(1)}, u32[]{:S(2)}) copy-start(f32[32,256]{1,0:T(8,128)S(1)} %multiply_add_fusion) | copy-start | bytes 98308
  117.2 11.1 %copy-start.12 = (s32[32,2]{0,1:T(2,128)S(1)}, s32[32,2]{0,1:T(2,128)}, u32[]{:S(2)}) copy-start(s32[32,2]{0,1:T(2,128)} %param.34) | copy-start | bytes 772
  117.2 11.1 %copy-start.14 = (s32[32,2]{0,1:T(2,128)S(1)}, s32[32,2]{0,1:T(2,128)}, u32[]{:S(2)}) copy-start(s32[32,2]{0,1:T(2,128)} %copy.95) | copy-start | bytes 772
  121.8 14.7 %all-to-all-start = ((bf16[16,32,256]{2,1,0:T(8,128)(2,1)}), bf16[16,32,256]{2,1,0:T(8,128)(2,1)S(1)}, u32[]{:S(2)}, u32[]{:S(2)}) async-start(bf16[16,32,256]{2,1,0:T(8,128)(2,1)} %bitcast.77), calls=%async_computation | async-start | bytes 524288 | tf_op jit(solution)/shard_map/all_to_all | solution.py:16
  128.4 30.7 %copy-start.16 = (s32[32]{0:T(128)}, s32[32]{0:T(128)S(1)}, u32[]{:S(2)}) copy-start(s32[32]{0:T(128)S(1)} %get-tuple-element.10) | copy-start | bytes 388
  128.4 30.7 %copy-start.18 = (s32[32]{0:T(128)}, s32[32]{0:T(128)S(1)}, u32[]{:S(2)}) copy-start(s32[32]{0:T(128)S(1)} %get-tuple-element.11) | copy-start | bytes 388
  157.9 4.9 %copy-start.3 = (bf16[128,32,128]{2,0,1:T(8,128)(2,1)S(1)}, bf16[128,32,128]{2,0,1:T(8,128)(2,1)}, u32[]{:S(2)}) copy-start(bf16[128,32,128]{2,0,1:T(8,128)(2,1)} %get-tuple-element.4) | copy-start | bytes 3145732
  159.1 21.9 %all-to-all-start.2 = ((bf16[16,160,256]{2,1,0:T(8,128)(2,1)}), bf16[16,160,256]{2,1,0:T(8,128)(2,1)S(1)}, u32[]{:S(2)}, u32[]{:S(2)}) async-start(bf16[16,160,256]{2,1,0:T(8,128)(2,1)} %broadcast_in_dim.53), calls=%async_computation.2 | async-start | bytes 2621440 | tf_op jit(solution)/shard_map/all_to_all | solution.py:16
  181.2 0.7 copy-start.11
  181.9 1.2 copy-start.20
  183.1 1.2 copy-start.2
  184.7 3.1 %copy-start.1 = (bf16[32,128,128]{2,1,0:T(8,128)(2,1)S(1)}, bf16[32,128,128]{2,1,0:T(8,128)(2,1)}, u32[]{:S(2)}) copy-start(bf16[32,128,128]{2,1,0:T(8,128)(2,1)} %get-tuple-element.5) | copy-start | bytes 3145732
  191.8 5.9 %copy-start.13 = (bf16[4096]{0:T(1024)(128)(2,1)S(1)}, bf16[4096]{0:T(1024)(128)(2,1)}, u32[]{:S(2)}) copy-start(bf16[4096]{0:T(1024)(128)(2,1)} %param.41) | copy-start | bytes 24580
  191.8 5.9 %copy-start.21 = (bf16[4096,32]{0,1:T(8,128)(2,1)S(1)}, bf16[4096,32]{0,1:T(8,128)(2,1)}, u32[]{:S(2)}) copy-start(bf16[4096,32]{0,1:T(8,128)(2,1)} %param.33) | copy-start | bytes 786436
  193.1 22.0 %all-to-all-start.3 = ((bf16[16,160,256]{2,1,0:T(8,128)(2,1)}), bf16[16,160,256]{2,1,0:T(8,128)(2,1)}, u32[]{:S(2)}, u32[]{:S(2)}) async-start(bf16[16,160,256]{2,1,0:T(8,128)(2,1)} %bitcast.81), calls=%async_computation.3 | async-start | bytes 2621440 | tf_op jit(solution)/shard_map/all_to_all | solution.py:16
  197.7 44.5 %copy-start.17 = (s32[32]{0:T(128)S(1)}, s32[32]{0:T(128)}, u32[]{:S(2)}) copy-start(s32[32]{0:T(128)} %copy-done.16) | copy-start | bytes 388
  197.7 44.5 %copy-start.19 = (s32[32]{0:T(128)S(1)}, s32[32]{0:T(128)}, u32[]{:S(2)}) copy-start(s32[32]{0:T(128)} %copy-done.18) | copy-start | bytes 388
  217.2 25.0 %all-to-all-start.4 = ((bf16[32,4,256]{2,1,0:T(4,128)(2,1)}), bf16[32,4,256]{2,1,0:T(4,128)(2,1)S(1)}, u32[]{:S(2)}, u32[]{:S(2)}) async-start(bf16[32,4,256]{2,1,0:T(4,128)(2,1)} %reshape.112), calls=%async_computation.4 | async-start | bytes 131072 | tf_op jit(solution)/shard_map/all_to_all | solution.py:16
  243.2 11.1 %all-to-all-start.5 = ((bf16[16,32,256]{2,1,0:T(8,128)(2,1)}), bf16[16,32,256]{2,1,0:T(8,128)(2,1)S(1)}, u32[]{:S(2)}, u32[]{:S(2)}) async-start(bf16[16,32,256]{2,1,0:T(8,128)(2,1)} %broadcast_in_dim.61), calls=%async_computation.5 | async-start | bytes 524288 | tf_op jit(solution)/shard_map/all_to_all | solution.py:16
Sparse Core Ops, SparseCore 0:
  14.4 85.5 all-gather.2

commit v2 on v1

--- a/solution.py
+++ b/solution.py
@@ -1,11 +1,13 @@
 import jax
 import jax.numpy as jnp
 from jax import lax
+from jax.experimental import pallas as pl
+from jax.experimental.pallas import tpu as pltpu
 from jax.sharding import Mesh
 from jax.sharding import PartitionSpec as P
 
 TOP_K = 2
-EP = ("ep_0", "ep_1")
+EP = ("far", "near", "core")
 
 
 epsilon = 1e-06
@@ -18,11 +20,6 @@
 
 def copies_to_all(value, axis):
     return exchange(jnp.broadcast_to(value, (lax.axis_size(axis), *value.shape)), axis)
-
-
-def features_cut(rows, devices):
-    count, width = rows.shape
-    return rows.reshape(count, devices, width // devices).swapaxes(0, 1)
 
 
 def features_joined(pieces):
@@ -40,8 +37,147 @@
     return jnp.dot(left, right, preferred_element_type=jnp.float32)
 
 
-def lane_blocks(weight, lanes):
-    return [weight[:, at : at + lanes] for at in range(0, weight.shape[1], lanes)]
+def vmem():
+    return pl.BlockSpec(memory_space=pltpu.VMEM)
+
+
+def block_kernel(rows_ref, mine_ref, theirs_ref, out_ref):
+    blocks = rows_ref.shape[0] // 2
+    sources, items, _ = out_ref.shape
+    half = items // 2
+    for side in range(2):
+        rows = jnp.concatenate([rows_ref[2 * b + side] for b in range(blocks)], axis=1)
+        depth = rows.shape[1] // 2
+        sums = dot(rows[:, :depth], mine_ref[...]) + dot(rows[:, depth:], theirs_ref[...])
+        sums = sums.astype(jnp.bfloat16)
+        for source in range(sources):
+            out_ref[source, side * half : (side + 1) * half, :] = sums[source * half : (source + 1) * half]
+
+
+def block_product(rows, mine, theirs, far, items):
+    columns = mine.shape[1]
+    return pl.pallas_call(
+        block_kernel,
+        out_shape=jax.ShapeDtypeStruct((far, items, columns), jnp.bfloat16),
+        in_specs=[vmem()] * 3,
+        out_specs=vmem(),
+        compiler_params=pltpu.CompilerParams(vmem_limit_bytes=16 * 1024 * 1024),
+        cost_estimate=pl.CostEstimate(flops=4 * rows.size * columns, bytes_accessed=2 * (rows.size + 2 * mine.size), transcendentals=0),
+    )(rows, mine, theirs)
+
+
+ROOMY = 61 * 1024 * 1024
+
+
+def output_kernel(rows_ref, whole_hbm, out_ref, weight_ref, sems):
+    channels = rows_ref.shape[1]
+    chips = out_ref.shape[0]
+    steps = 4
+    owners = 2 * chips // steps
+    copies = [
+        pltpu.make_async_copy(
+            whole_hbm.at[pl.ds(i * owners, owners), pl.ds(0, channels)],
+            weight_ref.at[pl.ds(i * owners, owners)],
+            sems.at[i],
+        )
+        for i in range(steps)
+    ]
+    for copy in copies:
+        copy.start()
+    rows = rows_ref[...]
+    for z in range(chips):
+        if z % (chips // steps) == 0:
+            copies[z // (chips // steps)].wait()
+        weight = jnp.concatenate([weight_ref[2 * z], weight_ref[2 * z + 1]], axis=1)
+        out_ref[z] = dot(rows, weight).astype(jnp.bfloat16)
+
+
+def output_product(rows, whole):
+    owners, _, lanes = whole.shape
+    channels = rows.shape[1]
+    return pl.pallas_call(
+        output_kernel,
+        out_shape=jax.ShapeDtypeStruct((owners // 2, rows.shape[0], 2 * lanes), jnp.bfloat16),
+        in_specs=[vmem(), pl.BlockSpec(memory_space=pl.ANY)],
+        out_specs=vmem(),
+        scratch_shapes=[pltpu.VMEM((owners, channels, lanes), whole.dtype), pltpu.SemaphoreType.DMA((4,))],
+        compiler_params=pltpu.CompilerParams(vmem_limit_bytes=ROOMY),
+        cost_estimate=pl.CostEstimate(flops=2 * rows.size * owners * lanes, bytes_accessed=2 * owners * channels * lanes, transcendentals=0),
+    )(rows, whole)
+
+
+def experts_kernel(pieces_ref, gain_ref, gate_hbm, up_hbm, down_hbm, whole_hbm, out_ref, own_ref, gate_ref, up_ref, down_ref, dense_ref, sems):
+    chips, count, share = pieces_ref.shape
+    depth = share // 2
+    dense_at = whole_hbm.shape[1] - 3 * depth
+    owners = whole_hbm.shape[0]
+    copies = [
+        pltpu.make_async_copy(source, target, sems.at[i])
+        for i, (source, target) in enumerate(
+            (
+                (gate_hbm, gate_ref),
+                (up_hbm, up_ref),
+                (whole_hbm.at[pl.ds(0, owners), pl.ds(dense_at, 3 * depth)], dense_ref),
+                (down_hbm, down_ref),
+            )
+        )
+    ]
+    for copy in copies:
+        copy.start()
+    slots = count - own_ref.shape[0]
+    squares = jnp.zeros((count, share), jnp.float32)
+    for z in range(chips):
+        values = pieces_ref[z].astype(jnp.float32)
+        squares = squares + values * values
+    mean = jnp.sum(squares, axis=1, keepdims=True) / (chips * share)
+    inverse = lax.rsqrt(mean + epsilon)
+    for copy in copies[:2]:
+        copy.wait()
+    routed = jnp.zeros((slots, share), jnp.float32)
+    for z in range(chips):
+        at = pl.ds(z * share, share)
+        rows = (pieces_ref[z].astype(jnp.float32) * inverse * gain_ref[:, at]).astype(jnp.bfloat16)
+        routed = routed + dot(rows[:slots], jnp.concatenate([gate_ref[at, :], up_ref[at, :]], axis=1))
+        own_ref[:, at] = rows[slots:]
+    half = share // 2
+    routed_act = (jax.nn.silu(routed[:, :half]) * routed[:, half:]).astype(jnp.bfloat16)
+    copies[2].wait()
+    dense = jnp.zeros((count - slots, share), jnp.float32)
+    for z in range(chips):
+        maps = [
+            jnp.concatenate([dense_ref[2 * z + c, i * depth : (i + 1) * depth] for c in range(2)], axis=0)
+            for i in range(2)
+        ]
+        dense = dense + dot(own_ref[:, pl.ds(z * share, share)], jnp.concatenate(maps, axis=1))
+    dense_act = (jax.nn.silu(dense[:, :half]) * dense[:, half:]).astype(jnp.bfloat16)
+    copies[3].wait()
+    for z in range(chips):
+        out_ref[z, :slots, :] = dot(routed_act, down_ref[:, pl.ds(z * share, share)]).astype(jnp.bfloat16)
+        weight = jnp.concatenate([dense_ref[2 * z + c, 2 * depth :] for c in range(2)], axis=1)
+        out_ref[z, slots:, :] = dot(dense_act, weight).astype(jnp.bfloat16)
+
+
+def experts_product(pieces, gain, gate, up, down, whole, own_rows):
+    chips, count, share = pieces.shape
+    owners, _, lanes = whole.shape
+    anywhere = pl.BlockSpec(memory_space=pl.ANY)
+    weights = (gate, up, down)
+    return pl.pallas_call(
+        experts_kernel,
+        out_shape=(
+            jax.ShapeDtypeStruct(pieces.shape, jnp.bfloat16),
+            jax.ShapeDtypeStruct((own_rows, chips * share), jnp.bfloat16),
+        ),
+        in_specs=[vmem(), vmem(), *([anywhere] * 4)],
+        out_specs=(vmem(), vmem()),
+        scratch_shapes=[
+            *(pltpu.VMEM(w.shape, w.dtype) for w in weights),
+            pltpu.VMEM((owners, 3 * lanes, lanes), whole.dtype),
+            pltpu.SemaphoreType.DMA((4,)),
+        ],
+        compiler_params=pltpu.CompilerParams(vmem_limit_bytes=ROOMY),
+        cost_estimate=pl.CostEstimate(flops=6 * count * gate.size, bytes_accessed=12 * gate.size, transcendentals=0),
+    )(pieces, gain, *weights, whole)
 
 
 def on_device(
@@ -69,25 +205,34 @@
 ):
     batch_rows, width = tokens.shape
     depth, channels = in_weight.shape
-    lanes = out_weight.shape[1]
     columns = lax.axis_size("tp")
     share = width // columns
-    parts = [*lane_blocks(in_weight, lanes), *lane_blocks(gate_weight, lanes), out_weight, dense_gate, dense_up, dense_down]
-    whole = lax.all_gather(jnp.concatenate(parts, axis=0), EP)
-    pieces, at = [], 0
-    for part in parts:
-        pieces.append(whole[:, at : at + part.shape[0]])
-        at += part.shape[0]
-    per = channels // lanes
-    by_rows = lambda piece: piece.reshape(-1, lanes)
-    by_columns = lambda piece: piece.swapaxes(0, 1).reshape(piece.shape[1], -1)
-    in_whole = jnp.concatenate([by_rows(p) for p in pieces[:per]], axis=1)
-    gate_whole = jnp.concatenate([by_rows(p) for p in pieces[per : 2 * per]], axis=1)
-    out_piece, dense_gate_piece, dense_up_piece, dense_down_piece = pieces[2 * per :]
-
+    far, near = lax.axis_size("far"), lax.axis_size("near")
+    core = lax.axis_index("core")
+    column = lax.axis_index("tp")
+    swap = lambda value: lax.ppermute(value, "core", [(0, 1), (1, 0)])
+    whole = lax.all_gather(jnp.concatenate([out_weight, dense_gate, dense_up, dense_down], axis=0), EP)
     normed = rms_scale(tokens, mix_gain)
-    x_branch = dot(normed, in_whole).astype(jnp.bfloat16)
-    gate_branch = dot(normed, gate_whole).astype(jnp.bfloat16)
+    half = batch_rows // 2
+    split_rows = normed.reshape(2, half, far, near, 2, depth)
+    block, side = column // 2, column % 2
+    block_near = (lax.axis_index("near") + block % near) % near
+    block_core = jnp.where(block < near, core, 1 - core)
+    sent = lax.dynamic_slice(
+        split_rows, (side, 0, 0, block_near, block_core, 0), (1, half, far, 1, 1, depth)
+    ).reshape(half, far, depth)
+    came = exchange(sent.swapaxes(0, 1), "far").reshape(far * half, depth)
+    block_rows = copies_to_all(came, "tp")
+    both_weights = jnp.concatenate([in_weight, gate_weight], axis=1)
+    from_near = lambda k: lax.ppermute(both_weights, "near", [(i, (i - k) % near) for i in range(near)])
+    others = [from_near(k) for k in range(1, near)]
+    block_mine = jnp.concatenate([both_weights, *others], axis=0)
+    block_theirs = swap(block_mine)
+    partial_sums = block_product(block_rows, block_mine, block_theirs, far, batch_rows)
+    sent_back = exchange(partial_sums, "far")
+    both_sums = sent_back.astype(jnp.float32).sum(axis=0)
+    x_branch = both_sums[:, :channels].astype(jnp.bfloat16)
+    gate_branch = both_sums[:, channels:].astype(jnp.bfloat16)
     window = jnp.concatenate([conv_state, x_branch[:, None, :]], axis=1)
     conv_out = jnp.sum(window.astype(jnp.float32) * conv_taps[None], axis=1).astype(jnp.bfloat16)
     new_conv_state = window[:, 1:, :]
@@ -104,10 +249,9 @@
         -jnp.expm1(2.0 * log_decay)
     ) * input_gate * conv_out.astype(jnp.float32)
     mixer_rows = (new_state * jax.nn.gelu(gate_branch.astype(jnp.float32))).astype(jnp.bfloat16)
-    mixer_part = dot(mixer_rows, by_columns(out_piece)).astype(jnp.bfloat16)
-
-    mixed_share = exchange(features_cut(mixer_part, columns), "tp").astype(jnp.float32).sum(axis=0)
-    own_tokens = lax.dynamic_slice_in_dim(tokens, lax.axis_index("tp") * share, share, 1)
+    own_tokens = lax.dynamic_slice_in_dim(tokens, column * share, share, 1)
+    mixer_part = output_product(mixer_rows, whole)
+    mixed_share = exchange(mixer_part, "tp").astype(jnp.float32).sum(axis=0)
     resid_share = (own_tokens.astype(jnp.float32) + mixed_share).astype(jnp.bfloat16)
 
     experts = router_weight.shape[1]
@@ -128,18 +272,16 @@
     arrived = exchange(outgoing, EP)
     sources, items, _ = arrived.shape
     slots = sources * items
-    both = jnp.concatenate([arrived.reshape(slots, share), resid_share], axis=0)
-    all_rows = features_joined(copies_to_all(both, "tp"))
-    all_normed = rms_scale(all_rows, ffn_gain)
-    rows, normed_ffn = all_normed[:slots], all_normed[slots:]
-
-    act = (jax.nn.silu(dot(rows, expert_gate[0])) * dot(rows, expert_up[0])).astype(jnp.bfloat16)
-    expert_part = dot(act, expert_down[0]).astype(jnp.bfloat16)
-    dense_first = dot(normed_ffn, by_rows(dense_gate_piece))
-    dense_second = dot(normed_ffn, by_rows(dense_up_piece))
-    dense_act = (jax.nn.silu(dense_first) * dense_second).astype(jnp.bfloat16)
-    dense_part = dot(dense_act, by_columns(dense_down_piece)).astype(jnp.bfloat16)
-    parts_cut = features_cut(jnp.concatenate([expert_part, dense_part], axis=0), columns)
+    shares = jnp.concatenate([arrived.reshape(slots, share), resid_share], axis=0)
+    parts_cut, normed_ffn = experts_product(
+        copies_to_all(shares, "tp"),
+        ffn_gain.reshape(1, width),
+        expert_gate[0],
+        expert_up[0],
+        expert_down[0],
+        whole,
+        batch_rows,
+    )
     sums = exchange(parts_cut, "tp").astype(jnp.float32).sum(axis=0)
     total, dense_share = sums[:slots].astype(jnp.bfloat16), sums[slots:]
 
@@ -168,7 +310,7 @@
 
 
 def solution(mesh):
-    split = Mesh(mesh.devices.reshape(16, 2, mesh.shape["tp"]), ("ep_0", "ep_1", "tp"))
+    split = Mesh(mesh.devices.reshape(4, 4, 2, mesh.shape["tp"]), (*EP, "tp"))
     in_specs = (
         P(EP, None),
         P(EP, "tp"),
@@ -193,6 +335,5 @@
         P(),
     )
     out_specs = (P(EP, None), P(EP, "tp"), P(EP, None, "tp"))
-    return jax.shard_map(
-        on_device, mesh=split, in_specs=in_specs, out_specs=out_specs, check_vma=False
-    )
+
+    return jax.shard_map(on_device, mesh=split, in_specs=in_specs, out_specs=out_specs, check_vma=False)

time: 264 us -> 227 us (0.86)
  waiting for transfers between devices: 143 us -> 69.9 us
  blocking collectives: 21 us -> 67.7 us
  local copies, waits for them, and re-layouts: 30.5 us -> 5.85 us
  starting transfers between devices: 30.3 us -> 50.5 us
  matrix products: 14.1 us -> 1.02 us
  Pallas kernels: 0 us -> 10.6 us
  other arithmetic: 8.27 us -> 5.02 us
    all_gather x1, waiting for transfers between devices: 81.4 us -> 0.5 us  [on_device(): lax.all_gather(jnp.concatenate([out_weight, dense_gate, dense_up, dense_d...]
    all_to_all x1 -> x3, blocking collectives: 21 us -> 67.7 us  [exchange(): return lax.all_to_all(pieces, axis, split_axis=0, concat_axis=0, tiled=True)]
    ppermute x0 -> x4, starting transfers between devices: none -> 16.6 us  [the longest x3 11.2 us: on_device(): lax.ppermute(both_weights, 'near', [(i, (i - k) % near) for i in range(ne...]
    dot_general x10 -> x4, matrix products: 12.1 us -> 0.72 us  [dot(): return jnp.dot(left, right, preferred_element_type=jnp.float32)]
    pallas_call x0 -> x3, Pallas kernels: none -> 10.6 us  [the longest x1 6.18 us: experts_product(): pl.pallas_call(experts_kernel, out_shape=(jax.ShapeDtypeStruct(pieces.sha...]
    unnamed x57 -> x27, local copies, waits for them, and re-layouts: 9.01 us -> 1.01 us
    slice x1 -> x0, local copies, waits for them, and re-layouts: 6.67 us -> none  [on_device(): pieces.append(whole[:, at:at + part.shape[0]])]
    transpose x3 -> x0, local copies, waits for them, and re-layouts: 6 us -> none  [on_device(): by_columns = lambda piece: piece.swapaxes(0, 1).reshape(piece.shape[1], -1)]
  transfers between devices with their start and end apart: 6 -> 11, of which waited for: 6 -> 9; matrix products, arithmetic and copies ran while one was open for 3% -> 3% of each run, Pallas kernels for 0% -> 1%
where the time goes in v2:
time: 227 us; the launch traced here: 225 us
  waiting for transfers between devices  69.9 us (31%)
  blocking collectives  67.7 us (30%)
  starting transfers between devices  50.5 us (22%)
  between operations  14.5 us (6%)
  Pallas kernels  10.6 us (5%)
  local copies, waits for them, and re-layouts  5.85 us (3%)
  other arithmetic  5.02 us (2%)
    all_to_all x3, blocking collectives, exchange(): return lax.all_to_all(pieces, axis, split_axis=0, concat_axis=0, tiled=True)  67.7 us
    all_to_all x6, waiting for transfers between devices, exchange(): return lax.all_to_all(pieces, axis, split_axis=0, concat_axis=0, tiled=True)  64.4 us
    all_to_all x6, starting transfers between devices, exchange(): return lax.all_to_all(pieces, axis, split_axis=0, concat_axis=0, tiled=True)  33.9 us
    ppermute x3, starting transfers between devices, on_device(): lax.ppermute(both_weights, 'near', [(i, (i - k) % near) for i in range(ne...  11.2 us
    pallas_call x1, Pallas kernels, experts_product(): pl.pallas_call(experts_kernel, out_shape=(jax.ShapeDtypeStruct(pieces.sha...  6.18 us
    ppermute x1, starting transfers between devices, on_device(): swap = lambda value: lax.ppermute(value, 'core', [(0, 1), (1, 0)])  5.41 us
    ppermute x3, waiting for transfers between devices, on_device(): lax.ppermute(both_weights, 'near', [(i, (i - k) % near) for i in range(ne...  4.91 us
  transfers between devices with their start and end apart: 11, of which 9 were waited for; matrix products, arithmetic and copies ran while one was open for 3% of the time, Pallas kernels for 1%

profile of v2, /device:TPU:1, one launch (start us, length us, event | category | flops | bytes accessed | tf_op | source)
XLA Modules:
  0.0 225.1 jit_solution(14602475889478473456)
XLA Ops:
  7.2 1.6 pad_maximum_fusion.1
  8.9 0.8 constant_dynamic-update-slice_fusion.1
  9.7 0.8 constant_dynamic-update-slice_fusion
  10.6 7.1 %collective-permute-start = (bf16[128,512]{1,0:T(8,128)(2,1)S(1)}, bf16[128,512]{1,0:T(8,128)(2,1)S(1)}, u32[]{:S(2)}, u32[]{:S(2)}) collective-permute-start(bf16[128,512]{1,0:T(8,128)(2,1)S(1)} %constant_dynamic-update-slice_fusion), channel_id=1, source_target_pairs={{0,96},{32,0},{64,32},{96,64},{1,97},{33,1},{65,33},{97,65},{2,98}... | collective-permute-start | bytes 393224 | tf_op jit(solution)/shard_map/ppermute | solution.py:227
  17.6 1.9 collective-permute-start.1
  19.6 2.2 collective-permute-start.2
  21.8 1.1 fusion.14
  22.9 1.5 collective-permute-done.1
  24.4 3.5 %collective-permute-done.2 = bf16[128,512]{1,0:T(8,128)(2,1)S(1)} collective-permute-done((bf16[128,512]{1,0:T(8,128)(2,1)S(1)}, bf16[128,512]{1,0:T(8,128)(2,1)S(1)}, u32[]{:S(2)}, u32[]{:S(2)}) %collective-permute-start.2) | collective-permute-done | bytes 131104 | tf_op jit(solution)/shard_map/ppermute | solution.py:227
  27.9 5.4 %collective-permute-start.3 = (bf16[512,512]{1,0:T(8,128)(2,1)S(1)}, bf16[512,512]{1,0:T(8,128)(2,1)S(1)}, u32[]{:S(2)}, u32[]{:S(2)}) collective-permute-start(bf16[512,512]{1,0:T(8,128)(2,1)S(1)} %pad_maximum_fusion.mine_ref), channel_id=1, source_target_pairs={{0,16},{16,0},{1,17},{17,1},{2,18},{18,2},{3,19},{19,3},{4,20},{20... | collective-permute-start | bytes 1572872 | tf_op jit(solution)/shard_map/ppermute | solution.py:213
  33.3 0.1 fusion.16
  33.5 0.2 reshape.70
  33.8 23.8 %all_to_all.45 = bf16[4,16,128]{2,1,0:T(8,128)(2,1)S(1)} all-to-all(bf16[4,16,128]{2,1,0:T(8,128)(2,1)S(1)} %bitcast.53), channel_id=1, replica_groups=mesh['far'=4,'near'=4,'core'=2,'tp'=16] {'far'}, dimensions={0} | all-to-all | bytes 32768 | tf_op jit(solution)/shard_map/all_to_all | solution.py:18
  57.6 0.8 broadcast_in_dim.53
  58.3 6.9 %all-to-all-start.1 = ((bf16[16,64,128]{2,1,0:T(8,128)(2,1)}), bf16[16,64,128]{2,1,0:T(8,128)(2,1)S(1)}, u32[]{:S(2)}, u32[]{:S(2)}) async-start(bf16[16,64,128]{2,1,0:T(8,128)(2,1)} %broadcast_in_dim.53), calls=%async_computation.1 | async-start | bytes 524288 | tf_op jit(solution)/shard_map/all_to_all | solution.py:18
  65.4 7.5 %all-to-all-done.1.rows_ref = bf16[16,64,128]{2,1,0:T(8,128)(2,1)S(1)} async-done(((bf16[16,64,128]{2,1,0:T(8,128)(2,1)}), bf16[16,64,128]{2,1,0:T(8,128)(2,1)S(1)}, u32[]{:S(2)}, u32[]{:S(2)}) %all-to-all-start.1) | async-done | bytes 262176 | tf_op jit(solution)/shard_map/all_to_all | solution.py:18
  72.9 1.1 shard_map.220
  74.0 3.5 %all-to-all-start.2 = ((bf16[4,32,512]{2,1,0:T(8,128)(2,1)}), bf16[4,32,512]{2,1,0:T(8,128)(2,1)S(1)}, u32[]{:S(2)}, u32[]{:S(2)}) async-start(bf16[4,32,512]{2,1,0:T(8,128)(2,1)} %shard_map.220), calls=%async_computation.2 | async-start | bytes 262144 | tf_op jit(solution)/shard_map/all_to_all | solution.py:18
  77.7 0.2 select_reduce_fusion.1
  77.9 0.1 reduce_sum.70
  78.0 12.3 %all-to-all-done.2 = bf16[4,32,512]{2,1,0:T(8,128)(2,1)S(1)} async-done(((bf16[4,32,512]{2,1,0:T(8,128)(2,1)}), bf16[4,32,512]{2,1,0:T(8,128)(2,1)S(1)}, u32[]{:S(2)}, u32[]{:S(2)}) %all-to-all-start.2) | async-done | bytes 131104 | tf_op jit(solution)/shard_map/all_to_all | solution.py:18
  90.5 0.2 fusion.7
  90.8 0.2 fusion.3
  91.1 0.7 fusion.26
  91.8 0.5 all-gather.3.cloned.1.call-done
  92.3 3.3 %shard_map.221 = bf16[16,32,256]{2,1,0:T(8,128)(2,1)} custom-call(bf16[32,256]{1,0:T(8,128)(2,1)} %get-tuple-element.7.rows_ref, bf16[32,640,128]{2,1,0:T(8,128)(2,1)} %bitcast.46), custom_call_target="tpu_custom_call" | custom-call | flops 67108864 | bytes 2097152 | tf_op jit(solution)/shard_map/pallas_call | solution.py:98
  95.6 7.4 %all-to-all-start.3 = ((bf16[16,32,256]{2,1,0:T(8,128)(2,1)}), bf16[16,32,256]{2,1,0:T(8,128)(2,1)S(1)}, u32[]{:S(2)}, u32[]{:S(2)}) async-start(bf16[16,32,256]{2,1,0:T(8,128)(2,1)} %shard_map.221), calls=%async_computation.3 | async-start | bytes 524288 | tf_op jit(solution)/shard_map/all_to_all | solution.py:18
  103.0 8.2 %all-to-all-done.3 = bf16[16,32,256]{2,1,0:T(8,128)(2,1)S(1)} async-done(((bf16[16,32,256]{2,1,0:T(8,128)(2,1)}), bf16[16,32,256]{2,1,0:T(8,128)(2,1)S(1)}, u32[]{:S(2)}, u32[]{:S(2)}) %all-to-all-start.3) | async-done | bytes 262176 | tf_op jit(solution)/shard_map/all_to_all | solution.py:18
  111.3 0.1 convolution_convert_fusion
  111.5 22.3 %all_to_all.46 = bf16[32,4,256]{2,1,0:T(4,128)(2,1)S(1)} all-to-all(bf16[32,4,256]{2,1,0:T(4,128)(2,1)S(1)} %reshape.73), channel_id=1, replica_groups=mesh['far'=4,'near'=4,'core'=2,'tp'=16] {'far','near','core'}, dimensions={0} | all-to-all | bytes 131072 | tf_op jit(solution)/shard_map/all_to_all | solution.py:18
  133.8 0.1 broadcast_in_dim.55
  133.9 21.6 %all_to_all.47.pieces_ref = bf16[16,160,256]{2,1,0:T(8,128)(2,1)} all-to-all(bf16[16,160,256]{2,1,0:T(8,128)(2,1)S(1)} %broadcast_in_dim.55), channel_id=1, replica_groups=mesh['far'=4,'near'=4,'core'=2,'tp'=16] {'tp'}, dimensions={0} | all-to-all | bytes 2621440 | tf_op jit(solution)/shard_map/all_to_all | solution.py:18
  155.5 6.2 %shard_map.222 = (bf16[16,160,256]{2,1,0:T(8,128)(2,1)}, bf16[32,4096]{1,0:T(8,128)(2,1)}) custom-call(bf16[16,160,256]{2,1,0:T(8,128)(2,1)} %all_to_all.47.pieces_ref, f32[1,4096]{1,0:T(1,128)} %bitcast.55, bf16[4096,128]{1,0:T(8,128)(2,1)} %bitcast.48, bf16[4096,128]{1,0:T(8,128)(2,1)} %bitcast.49, bf16[128,4096]{1,0:T(8,128)(2,1)} %bitcast.50, ...), custom_call_target="tpu_custom_call" | custom-call | flops 503316480 | bytes 6291456 | tf_op jit(solution)/shard_map/pallas_call | solution.py:165
  161.7 3.8 %all-to-all-start.6 = ((bf16[16,160,256]{2,1,0:T(8,128)(2,1)}), bf16[16,160,256]{2,1,0:T(8,128)(2,1)S(1)}, u32[]{:S(2)}, u32[]{:S(2)}) async-start(bf16[16,160,256]{2,1,0:T(8,128)(2,1)} %get-tuple-element.6), calls=%async_computation.6 | async-start | bytes 2621440 | tf_op jit(solution)/shard_map/all_to_all | solution.py:18
  165.6 0.2 fusion.47
  165.8 0.2 select_reduce_fusion
  166.1 16.8 %all-to-all-done.6 = bf16[16,160,256]{2,1,0:T(8,128)(2,1)S(1)} async-done(((bf16[16,160,256]{2,1,0:T(8,128)(2,1)}), bf16[16,160,256]{2,1,0:T(8,128)(2,1)S(1)}, u32[]{:S(2)}, u32[]{:S(2)}) %all-to-all-start.6) | async-done | bytes 1310752 | tf_op jit(solution)/shard_map/all_to_all | solution.py:18
  182.9 0.2 convert_reduce_fusion
  183.1 0.7 reshape.76
  183.7 8.8 %all-to-all-start.7 = ((bf16[32,4,256]{2,1,0:T(4,128)(2,1)}), bf16[32,4,256]{2,1,0:T(4,128)(2,1)S(1)}, u32[]{:S(2)}, u32[]{:S(2)}) async-start(bf16[32,4,256]{2,1,0:T(4,128)(2,1)} %reshape.76), calls=%async_computation.7 | async-start | bytes 131072 | tf_op jit(solution)/shard_map/all_to_all | solution.py:18
  192.5 0.2 fusion.13
  192.7 12.8 %all-to-all-done.7 = bf16[32,4,256]{2,1,0:T(4,128)(2,1)S(1)} async-done(((bf16[32,4,256]{2,1,0:T(4,128)(2,1)}), bf16[32,4,256]{2,1,0:T(4,128)(2,1)S(1)}, u32[]{:S(2)}, u32[]{:S(2)}) %all-to-all-start.7) | async-done | bytes 65568 | tf_op jit(solution)/shard_map/all_to_all | solution.py:18
  205.5 0.2 fusion.9
  205.7 0.7 broadcast_in_dim.63
  206.5 3.5 %all-to-all-start.8 = ((bf16[16,32,256]{2,1,0:T(8,128)(2,1)}), bf16[16,32,256]{2,1,0:T(8,128)(2,1)S(1)}, u32[]{:S(2)}, u32[]{:S(2)}) async-start(bf16[16,32,256]{2,1,0:T(8,128)(2,1)} %broadcast_in_dim.63), calls=%async_computation.8 | async-start | bytes 524288 | tf_op jit(solution)/shard_map/all_to_all | solution.py:18
  210.0 0.6 fusion.19
  210.6 6.9 %all-to-all-done.8 = bf16[16,32,256]{2,1,0:T(8,128)(2,1)S(1)} async-done(((bf16[16,32,256]{2,1,0:T(8,128)(2,1)}), bf16[16,32,256]{2,1,0:T(8,128)(2,1)S(1)}, u32[]{:S(2)}, u32[]{:S(2)}) %all-to-all-start.8) | async-done | bytes 262176 | tf_op jit(solution)/shard_map/all_to_all | solution.py:18
  217.5 0.7 copy.85
  (59 shorter events, 1.3 us)
Async XLA Ops:
  7.2 158.5 %copy-start = (bf16[4096,32]{0,1:T(8,128)(2,1)S(1)}, bf16[4096,32]{0,1:T(8,128)(2,1)}, u32[]{:S(2)}) copy-start(bf16[4096,32]{0,1:T(8,128)(2,1)} %param.33) | copy-start | bytes 786436
  7.2 26.1 %copy-start.1 = (bf16[32,4096]{1,0:T(8,128)(2,1)S(1)}, bf16[32,4096]{1,0:T(8,128)(2,1)}, u32[]{:S(2)}) copy-start(bf16[32,4096]{1,0:T(8,128)(2,1)} %param.21) | copy-start | bytes 786436
  7.2 26.1 %copy-start.5 = (f32[4096]{0:T(1024)S(1)}, f32[4096]{0:T(1024)}, u32[]{:S(2)}) copy-start(f32[4096]{0:T(1024)} %param.24) | copy-start | bytes 49156
  7.2 85.1 %all-gather.3.cloned.1.call-start = ((), (), s32[]{:S(2)}) async-start(), calls=%async_computation.9 | async-start | bytes 5406720 | tf_op jit(solution)/shard_map/all_gather | solution.py:214
  10.6 12.3 %collective-permute-start = (bf16[128,512]{1,0:T(8,128)(2,1)S(1)}, bf16[128,512]{1,0:T(8,128)(2,1)S(1)}, u32[]{:S(2)}, u32[]{:S(2)}) collective-permute-start(bf16[128,512]{1,0:T(8,128)(2,1)S(1)} %constant_dynamic-update-slice_fusion), channel_id=1, source_target_pairs={{0,96},{32,0},{64,32},{96,64},{1,97},{33,1},{65,33},{97,65},{2,98}... | collective-permute-start | bytes 393224 | tf_op jit(solution)/shard_map/ppermute | solution.py:227
  17.6 6.7 %collective-permute-start.1 = (bf16[128,512]{1,0:T(8,128)(2,1)S(1)}, bf16[128,512]{1,0:T(8,128)(2,1)S(1)}, u32[]{:S(2)}, u32[]{:S(2)}) collective-permute-start(bf16[128,512]{1,0:T(8,128)(2,1)S(1)} %constant_dynamic-update-slice_fusion), channel_id=1, source_target_pairs={{0,64},{32,96},{64,0},{96,32},{1,65},{33,97},{65,1},{97,33},{2,66}... | collective-permute-start | bytes 393224 | tf_op jit(solution)/shard_map/ppermute | solution.py:227
  19.6 8.2 %collective-permute-start.2 = (bf16[128,512]{1,0:T(8,128)(2,1)S(1)}, bf16[128,512]{1,0:T(8,128)(2,1)S(1)}, u32[]{:S(2)}, u32[]{:S(2)}) collective-permute-start(bf16[128,512]{1,0:T(8,128)(2,1)S(1)} %constant_dynamic-update-slice_fusion), channel_id=1, source_target_pairs={{0,32},{32,64},{64,96},{96,0},{1,33},{33,65},{65,97},{97,1},{2,34}... | collective-permute-start | bytes 393224 | tf_op jit(solution)/shard_map/ppermute | solution.py:227
  27.9 37.4 %copy-start.6 = (s32[32,2]{0,1:T(2,128)S(1)}, s32[32,2]{0,1:T(2,128)}, u32[]{:S(2)}) copy-start(s32[32,2]{0,1:T(2,128)} %param.34) | copy-start | bytes 772
  27.9 45.0 %collective-permute-start.3 = (bf16[512,512]{1,0:T(8,128)(2,1)S(1)}, bf16[512,512]{1,0:T(8,128)(2,1)S(1)}, u32[]{:S(2)}, u32[]{:S(2)}) collective-permute-start(bf16[512,512]{1,0:T(8,128)(2,1)S(1)} %pad_maximum_fusion.mine_ref), channel_id=1, source_target_pairs={{0,16},{16,0},{1,17},{17,1},{2,18},{18,2},{3,19},{19,3},{4,20},{20... | collective-permute-start | bytes 1572872 | tf_op jit(solution)/shard_map/ppermute | solution.py:213
  57.6 20.5 %copy-start.9 = (f32[256]{0:T(256)S(1)}, f32[256]{0:T(256)}, u32[]{:S(2)}) copy-start(f32[256]{0:T(256)} %param.30) | copy-start | bytes 3076
  58.3 32.0 %copy-start.3 = (bf16[32,3,256]{2,0,1:T(8,128)(2,1)S(1)}, bf16[32,3,256]{2,0,1:T(8,128)(2,1)}, u32[]{:S(2)}) copy-start(bf16[32,3,256]{2,0,1:T(8,128)(2,1)} %param.23) | copy-start | bytes 147460
  58.3 32.0 %copy-start.8 = (f32[4,256]{1,0:T(4,128)S(1)}, f32[4,256]{1,0:T(4,128)}, u32[]{:S(2)}) copy-start(f32[4,256]{1,0:T(4,128)} %param.27) | copy-start | bytes 12292
  58.3 32.2 %copy-start.10 = (bf16[4,64,64]{2,1,0:T(8,128)(2,1)S(1)}, bf16[4,64,64]{2,1,0:T(8,128)(2,1)}, u32[]{:S(2)}) copy-start(bf16[4,64,64]{2,1,0:T(8,128)(2,1)} %param.28) | copy-start | bytes 98308
  58.3 14.6 %all-to-all-start.1 = ((bf16[16,64,128]{2,1,0:T(8,128)(2,1)}), bf16[16,64,128]{2,1,0:T(8,128)(2,1)S(1)}, u32[]{:S(2)}, u32[]{:S(2)}) async-start(bf16[16,64,128]{2,1,0:T(8,128)(2,1)} %broadcast_in_dim.53), calls=%async_computation.1 | async-start | bytes 524288 | tf_op jit(solution)/shard_map/all_to_all | solution.py:18
  65.4 25.4 %copy-start.11 = (bf16[4,64,64]{2,1,0:T(8,128)(2,1)S(1)}, bf16[4,64,64]{2,1,0:T(8,128)(2,1)}, u32[]{:S(2)}) copy-start(bf16[4,64,64]{2,1,0:T(8,128)(2,1)} %param.29) | copy-start | bytes 98308
  74.0 17.1 %copy-start.4 = (f32[32,256]{1,0:T(8,128)S(1)}, f32[32,256]{1,0:T(8,128)}, u32[]{:S(2)}) copy-start(f32[32,256]{1,0:T(8,128)} %param.22) | copy-start | bytes 98308
  74.0 16.3 %all-to-all-start.2 = ((bf16[4,32,512]{2,1,0:T(8,128)(2,1)}), bf16[4,32,512]{2,1,0:T(8,128)(2,1)S(1)}, u32[]{:S(2)}, u32[]{:S(2)}) async-start(bf16[4,32,512]{2,1,0:T(8,128)(2,1)} %shard_map.220), calls=%async_computation.2 | async-start | bytes 262144 | tf_op jit(solution)/shard_map/all_to_all | solution.py:18
  95.6 15.6 %all-to-all-start.3 = ((bf16[16,32,256]{2,1,0:T(8,128)(2,1)}), bf16[16,32,256]{2,1,0:T(8,128)(2,1)S(1)}, u32[]{:S(2)}, u32[]{:S(2)}) async-start(bf16[16,32,256]{2,1,0:T(8,128)(2,1)} %shard_map.221), calls=%async_computation.3 | async-start | bytes 524288 | tf_op jit(solution)/shard_map/all_to_all | solution.py:18
  161.7 3.9 %copy-start.7 = (bf16[4096]{0:T(1024)(128)(2,1)S(1)}, bf16[4096]{0:T(1024)(128)(2,1)}, u32[]{:S(2)}) copy-start(bf16[4096]{0:T(1024)(128)(2,1)} %param.41) | copy-start | bytes 24580
  161.7 3.9 %copy-start.2 = (bf16[32,4096]{1,0:T(8,128)(2,1)S(1)}, bf16[32,4096]{1,0:T(8,128)(2,1)}, u32[]{:S(2)}) copy-start(bf16[32,4096]{1,0:T(8,128)(2,1)} %get-tuple-element.5) | copy-start | bytes 786436
  161.7 21.1 %all-to-all-start.6 = ((bf16[16,160,256]{2,1,0:T(8,128)(2,1)}), bf16[16,160,256]{2,1,0:T(8,128)(2,1)S(1)}, u32[]{:S(2)}, u32[]{:S(2)}) async-start(bf16[16,160,256]{2,1,0:T(8,128)(2,1)} %get-tuple-element.6), calls=%async_computation.6 | async-start | bytes 2621440 | tf_op jit(solution)/shard_map/all_to_all | solution.py:18
  183.7 21.8 %all-to-all-start.7 = ((bf16[32,4,256]{2,1,0:T(4,128)(2,1)}), bf16[32,4,256]{2,1,0:T(4,128)(2,1)S(1)}, u32[]{:S(2)}, u32[]{:S(2)}) async-start(bf16[32,4,256]{2,1,0:T(4,128)(2,1)} %reshape.76), calls=%async_computation.7 | async-start | bytes 131072 | tf_op jit(solution)/shard_map/all_to_all | solution.py:18
  206.5 11.1 %all-to-all-start.8 = ((bf16[16,32,256]{2,1,0:T(8,128)(2,1)}), bf16[16,32,256]{2,1,0:T(8,128)(2,1)S(1)}, u32[]{:S(2)}, u32[]{:S(2)}) async-start(bf16[16,32,256]{2,1,0:T(8,128)(2,1)} %broadcast_in_dim.63), calls=%async_computation.8 | async-start | bytes 524288 | tf_op jit(solution)/shard_map/all_to_all | solution.py:18
Sparse Core Ops, SparseCore 0:
  10.1 82.1 all-gather.2

commit v3 on v2

--- a/solution.py
+++ b/solution.py
@@ -66,7 +66,7 @@
     )(rows, mine, theirs)
 
 
-ROOMY = 61 * 1024 * 1024
+ROOMY = 60 * 1024 * 1024
 
 
 def output_kernel(rows_ref, whole_hbm, out_ref, weight_ref, sems):
@@ -106,78 +106,108 @@
     )(rows, whole)
 
 
-def experts_kernel(pieces_ref, gain_ref, gate_hbm, up_hbm, down_hbm, whole_hbm, out_ref, own_ref, gate_ref, up_ref, down_ref, dense_ref, sems):
-    chips, count, share = pieces_ref.shape
-    depth = share // 2
-    dense_at = whole_hbm.shape[1] - 3 * depth
-    owners = whole_hbm.shape[0]
+def fetch_kernel(gate_hbm, up_hbm, down_hbm, whole_hbm, both_ref, down_ref, dense_ref, sems):
+    half = gate_hbm.shape[1]
+    owners, rows, _ = dense_ref.shape
     copies = [
         pltpu.make_async_copy(source, target, sems.at[i])
         for i, (source, target) in enumerate(
             (
-                (gate_hbm, gate_ref),
-                (up_hbm, up_ref),
-                (whole_hbm.at[pl.ds(0, owners), pl.ds(dense_at, 3 * depth)], dense_ref),
+                (gate_hbm, both_ref.at[:, pl.ds(0, half)]),
+                (up_hbm, both_ref.at[:, pl.ds(half, half)]),
+                (whole_hbm.at[pl.ds(0, owners), pl.ds(whole_hbm.shape[1] - rows, rows)], dense_ref),
                 (down_hbm, down_ref),
             )
         )
     ]
     for copy in copies:
         copy.start()
-    slots = count - own_ref.shape[0]
+    for copy in copies:
+        copy.wait()
+
+
+def fetch_weights(gate, up, down, whole, dense_rows):
+    owners, _, lanes = whole.shape
+    return pl.pallas_call(
+        fetch_kernel,
+        out_shape=(
+            jax.ShapeDtypeStruct((gate.shape[0], 2 * gate.shape[1]), gate.dtype),
+            jax.ShapeDtypeStruct(down.shape, down.dtype),
+            jax.ShapeDtypeStruct((owners, dense_rows, lanes), whole.dtype),
+        ),
+        in_specs=[pl.BlockSpec(memory_space=pl.ANY)] * 4,
+        out_specs=(vmem(),) * 3,
+        scratch_shapes=[pltpu.SemaphoreType.DMA((4,))],
+        compiler_params=pltpu.CompilerParams(vmem_limit_bytes=54 * 1024 * 1024),
+        cost_estimate=pl.CostEstimate(flops=40_000_000, bytes_accessed=6 * gate.size, transcendentals=0),
+    )(gate, up, down, whole)
+
+
+def experts_kernel(pieces_ref, gain_ref, both_ref, down_ref, dense_ref, maps_ref, picks_ref, places_ref, out_ref, combine_ref, branch_ref):
+    chips, count, share = pieces_ref.shape
+    depth = share // 2
+    slots = down_ref.shape[0]
+    rows_own = count - slots
     squares = jnp.zeros((count, share), jnp.float32)
     for z in range(chips):
         values = pieces_ref[z].astype(jnp.float32)
         squares = squares + values * values
     mean = jnp.sum(squares, axis=1, keepdims=True) / (chips * share)
     inverse = lax.rsqrt(mean + epsilon)
-    for copy in copies[:2]:
-        copy.wait()
     routed = jnp.zeros((slots, share), jnp.float32)
+    dense = jnp.zeros((rows_own, share), jnp.float32)
+    logits = jnp.zeros((rows_own, maps_ref.shape[0]), jnp.float32)
     for z in range(chips):
         at = pl.ds(z * share, share)
         rows = (pieces_ref[z].astype(jnp.float32) * inverse * gain_ref[:, at]).astype(jnp.bfloat16)
-        routed = routed + dot(rows[:slots], jnp.concatenate([gate_ref[at, :], up_ref[at, :]], axis=1))
-        own_ref[:, at] = rows[slots:]
-    half = share // 2
-    routed_act = (jax.nn.silu(routed[:, :half]) * routed[:, half:]).astype(jnp.bfloat16)
-    copies[2].wait()
-    dense = jnp.zeros((count - slots, share), jnp.float32)
-    for z in range(chips):
-        maps = [
+        routed = routed + dot(rows[:slots], both_ref[at, :])
+        weights = [
             jnp.concatenate([dense_ref[2 * z + c, i * depth : (i + 1) * depth] for c in range(2)], axis=0)
             for i in range(2)
         ]
-        dense = dense + dot(own_ref[:, pl.ds(z * share, share)], jnp.concatenate(maps, axis=1))
+        dense = dense + dot(rows[slots:], jnp.concatenate(weights, axis=1))
+        logits = logits + lax.dot_general(
+            rows[slots:], maps_ref[:, at], (((1,), (1,)), ((), ())), preferred_element_type=jnp.float32
+        )
+    half = share // 2
+    routed_act = (jax.nn.silu(routed[:, :half]) * routed[:, half:]).astype(jnp.bfloat16)
     dense_act = (jax.nn.silu(dense[:, :half]) * dense[:, half:]).astype(jnp.bfloat16)
-    copies[3].wait()
     for z in range(chips):
         out_ref[z, :slots, :] = dot(routed_act, down_ref[:, pl.ds(z * share, share)]).astype(jnp.bfloat16)
         weight = jnp.concatenate([dense_ref[2 * z + c, 2 * depth :] for c in range(2)], axis=1)
         out_ref[z, slots:, :] = dot(dense_act, weight).astype(jnp.bfloat16)
 
-
-def experts_product(pieces, gain, gate, up, down, whole, own_rows):
-    chips, count, share = pieces.shape
-    owners, _, lanes = whole.shape
-    anywhere = pl.BlockSpec(memory_space=pl.ANY)
-    weights = (gate, up, down)
+    experts = maps_ref.shape[0] - 8
+    column = lax.broadcasted_iota(jnp.int32, logits.shape, 1)
+
+    def of_column(index):
+        return jnp.sum(jnp.where(column == index, logits, 0.0), axis=1, keepdims=True)
+
+    picked = [of_column(picks_ref[:, k : k + 1]) for k in range(TOP_K)]
+    place = lax.broadcasted_iota(jnp.int32, (rows_own, combine_ref.shape[1]), 1)
+    total = jnp.zeros((rows_own, combine_ref.shape[1]), jnp.float32)
+    for k in range(TOP_K):
+        weight = jax.nn.sigmoid(picked[k] - picked[1 - k]).astype(jnp.bfloat16).astype(jnp.float32)
+        total = total + jnp.where(place == places_ref[:, k : k + 1], weight, 0.0)
+    combine_ref[...] = total.astype(jnp.bfloat16)
+    branch_ref[...] = jnp.broadcast_to(jax.nn.sigmoid(of_column(experts)), branch_ref.shape)
+
+
+def experts_product(pieces, gain, both, down, dense, maps, picks, places):
+    _, count, share = pieces.shape
+    own_rows = picks.shape[0]
     return pl.pallas_call(
         experts_kernel,
         out_shape=(
             jax.ShapeDtypeStruct(pieces.shape, jnp.bfloat16),
-            jax.ShapeDtypeStruct((own_rows, chips * share), jnp.bfloat16),
+            jax.ShapeDtypeStruct((own_rows, count - own_rows), jnp.bfloat16),
+            jax.ShapeDtypeStruct((own_rows, share), jnp.float32),
         ),
-        in_specs=[vmem(), vmem(), *([anywhere] * 4)],
-        out_specs=(vmem(), vmem()),
-        scratch_shapes=[
-            *(pltpu.VMEM(w.shape, w.dtype) for w in weights),
-            pltpu.VMEM((owners, 3 * lanes, lanes), whole.dtype),
-            pltpu.SemaphoreType.DMA((4,)),
-        ],
-        compiler_params=pltpu.CompilerParams(vmem_limit_bytes=ROOMY),
-        cost_estimate=pl.CostEstimate(flops=6 * count * gate.size, bytes_accessed=12 * gate.size, transcendentals=0),
-    )(pieces, gain, *weights, whole)
+        in_specs=[vmem()] * 8,
+        out_specs=(vmem(),) * 3,
+        compiler_params=pltpu.CompilerParams(vmem_limit_bytes=16 * 1024 * 1024),
+        cost_estimate=pl.CostEstimate(flops=3 * count * both.size, bytes_accessed=6 * both.size, transcendentals=0),
+    )(pieces, gain, both, down, dense, maps, picks, places)
 
 
 def on_device(
@@ -222,6 +252,25 @@
         split_rows, (side, 0, 0, block_near, block_core, 0), (1, half, far, 1, 1, depth)
     ).reshape(half, far, depth)
     came = exchange(sent.swapaxes(0, 1), "far").reshape(far * half, depth)
+    experts = router_weight.shape[1]
+    capacity = 2 * batch_rows * TOP_K // experts
+    flat_ids = routes.reshape(batch_rows * TOP_K)
+    onehot = (
+        flat_ids[:, None] == lax.broadcasted_iota(jnp.int32, (batch_rows * TOP_K, experts), 1)
+    ).astype(jnp.int32)
+    rank = jnp.sum((jnp.cumsum(onehot, axis=0) - onehot) * onehot, axis=1)
+    slot_of = (flat_ids * capacity + rank).reshape(batch_rows, TOP_K)
+    slots = experts * capacity
+    slot_rows = lax.broadcasted_iota(jnp.int32, (slots, batch_rows), 0)
+    dispatch = sum((slot_rows == slot_of[None, :, pick]).astype(jnp.bfloat16) for pick in range(TOP_K))
+    maps = jnp.concatenate(
+        [router_weight.T, branch_gate.reshape(1, width), jnp.zeros((7, width), jnp.bfloat16)], axis=0
+    )
+    own_tokens = lax.dynamic_slice_in_dim(tokens, column * share, share, 1)
+    came, dispatch, slot_of, maps, own_tokens = lax.optimization_barrier(
+        (came, dispatch, slot_of, maps, own_tokens)
+    )
+
     block_rows = copies_to_all(came, "tp")
     both_weights = jnp.concatenate([in_weight, gate_weight], axis=1)
     from_near = lambda k: lax.ppermute(both_weights, "near", [(i, (i - k) % near) for i in range(near)])
@@ -249,61 +298,26 @@
         -jnp.expm1(2.0 * log_decay)
     ) * input_gate * conv_out.astype(jnp.float32)
     mixer_rows = (new_state * jax.nn.gelu(gate_branch.astype(jnp.float32))).astype(jnp.bfloat16)
-    own_tokens = lax.dynamic_slice_in_dim(tokens, column * share, share, 1)
+    mixer_rows, new_conv_state = lax.optimization_barrier((mixer_rows, new_conv_state))
     mixer_part = output_product(mixer_rows, whole)
     mixed_share = exchange(mixer_part, "tp").astype(jnp.float32).sum(axis=0)
     resid_share = (own_tokens.astype(jnp.float32) + mixed_share).astype(jnp.bfloat16)
 
-    experts = router_weight.shape[1]
-    capacity = 2 * batch_rows * TOP_K // experts
-    flat_ids = routes.reshape(batch_rows * TOP_K)
-    onehot = (
-        flat_ids[:, None] == lax.broadcasted_iota(jnp.int32, (batch_rows * TOP_K, experts), 1)
-    ).astype(jnp.int32)
-    rank = jnp.sum((jnp.cumsum(onehot, axis=0) - onehot) * onehot, axis=1)
-    slot_of = (flat_ids * capacity + rank).reshape(batch_rows, TOP_K)
-    slot_rows = lax.broadcasted_iota(jnp.int32, (experts * capacity, batch_rows), 0)
-    slot_cols = lax.broadcasted_iota(jnp.int32, (batch_rows, experts * capacity), 1)
-    dispatch = jnp.zeros((experts * capacity, batch_rows), jnp.bfloat16)
-    for pick in range(TOP_K):
-        dispatch = dispatch + (slot_rows == slot_of[None, :, pick]).astype(jnp.bfloat16)
-
-    outgoing = dot(dispatch, resid_share).astype(jnp.bfloat16).reshape(experts, capacity, share)
-    arrived = exchange(outgoing, EP)
-    sources, items, _ = arrived.shape
-    slots = sources * items
-    shares = jnp.concatenate([arrived.reshape(slots, share), resid_share], axis=0)
-    parts_cut, normed_ffn = experts_product(
-        copies_to_all(shares, "tp"),
-        ffn_gain.reshape(1, width),
-        expert_gate[0],
-        expert_up[0],
-        expert_down[0],
-        whole,
-        batch_rows,
+    outgoing = dot(dispatch, resid_share).astype(jnp.bfloat16)
+    arrived = exchange(outgoing.reshape(experts, capacity, share), EP).reshape(slots, share)
+    fetched = fetch_weights(expert_gate[0], expert_up[0], expert_down[0], whole, 3 * depth)
+    arrived, fetched = lax.optimization_barrier((arrived, fetched))
+    shares = jnp.concatenate([arrived, resid_share], axis=0)
+    parts_cut, combine, branch_weight = experts_product(
+        copies_to_all(shares, "tp"), ffn_gain.reshape(1, width), *fetched, maps, routes, slot_of
     )
     sums = exchange(parts_cut, "tp").astype(jnp.float32).sum(axis=0)
     total, dense_share = sums[:slots].astype(jnp.bfloat16), sums[slots:]
 
-    router_logits = dot(normed_ffn, router_weight)
-    expert_ids = lax.broadcasted_iota(jnp.int32, (batch_rows, TOP_K, experts), 2)
-    picked = jnp.sum(
-        jnp.where(routes[:, :, None] == expert_ids, router_logits[:, None, :], 0.0), axis=2
-    )
-    route_weight = jax.nn.sigmoid(picked - picked[:, ::-1]).astype(jnp.bfloat16)
-    combine = jnp.zeros((batch_rows, experts * capacity), jnp.bfloat16)
-    for pick in range(TOP_K):
-        combine = combine + jnp.where(
-            slot_cols == slot_of[:, pick : pick + 1],
-            route_weight[:, pick : pick + 1],
-            jnp.zeros((), jnp.bfloat16),
-        )
-    branch_weight = jax.nn.sigmoid(dot(normed_ffn, branch_gate))
-
-    returned = exchange(total.reshape(sources, items, share), EP)
-    moe = dot(combine, returned.reshape(experts * capacity, share))
+    returned = exchange(total.reshape(experts, capacity, share), EP)
+    moe = dot(combine, returned.reshape(slots, share))
     out_share = (
-        resid_share.astype(jnp.float32) + moe + branch_weight[:, None] * dense_share
+        resid_share.astype(jnp.float32) + moe + branch_weight * dense_share
     ).astype(jnp.bfloat16)
     layer_out = features_joined(copies_to_all(out_share, "tp"))
     return (layer_out, new_state, new_conv_state)

time: 227 us -> 223 us (0.982)
  waiting for transfers between devices: 69.9 us -> 34.6 us
  blocking collectives: 67.7 us -> 103 us
  starting transfers between devices: 50.5 us -> 43.9 us
    all_to_all x3 -> x6, blocking collectives: 67.7 us -> 103 us  [exchange(): return lax.all_to_all(pieces, axis, split_axis=0, concat_axis=0, tiled=True)]
    all_to_all x6 -> x3, waiting for transfers between devices: 64.4 us -> 29.8 us  [exchange(): return lax.all_to_all(pieces, axis, split_axis=0, concat_axis=0, tiled=True)]
    all_to_all x6 -> x3, starting transfers between devices: 33.9 us -> 28.2 us  [exchange(): return lax.all_to_all(pieces, axis, split_axis=0, concat_axis=0, tiled=True)]
    pallas_call x0 -> x1, Pallas kernels: none -> 5.48 us  [fetch_weights(): pl.pallas_call(fetch_kernel, out_shape=(jax.ShapeDtypeStruct((gate.shape[...]
    ppermute x3, waiting for transfers between devices: 4.91 us -> 0.01 us  [on_device(): lax.ppermute(both_weights, 'near', [(i, (i - k) % near) for i in range(ne...]
    pallas_call x1, Pallas kernels: 6.18 us -> 1.83 us  [experts_product(): pl.pallas_call(experts_kernel, out_shape=(jax.ShapeDtypeStruct(pieces.sha...]
    all_gather x1, waiting for transfers between devices: 0.5 us -> 4.82 us  [on_device(): lax.all_gather(jnp.concatenate([out_weight, dense_gate, dense_up, dense_d...]
  transfers between devices with their start and end apart: 11 -> 8, of which waited for: 9 -> 4; matrix products, arithmetic and copies ran while one was open for 3% -> 3% of each run, Pallas kernels for 1% -> 3%
where the time goes in v3:
time: 223 us; the launch traced here: 221 us
  blocking collectives  103 us (46%)
  starting transfers between devices  43.9 us (20%)
  waiting for transfers between devices  34.6 us (16%)
  between operations  14.5 us (7%)
  Pallas kernels  11.7 us (5%)
  local copies, waits for them, and re-layouts  6.85 us (3%)
  other arithmetic  5.74 us (3%)
    all_to_all x6, blocking collectives, exchange(): return lax.all_to_all(pieces, axis, split_axis=0, concat_axis=0, tiled=True)  103 us
    all_to_all x3, waiting for transfers between devices, exchange(): return lax.all_to_all(pieces, axis, split_axis=0, concat_axis=0, tiled=True)  29.8 us
    all_to_all x3, starting transfers between devices, exchange(): return lax.all_to_all(pieces, axis, split_axis=0, concat_axis=0, tiled=True)  28.2 us
    ppermute x3, starting transfers between devices, on_device(): lax.ppermute(both_weights, 'near', [(i, (i - k) % near) for i in range(ne...  11.9 us
    pallas_call x1, Pallas kernels, fetch_weights(): pl.pallas_call(fetch_kernel, out_shape=(jax.ShapeDtypeStruct((gate.shape[...  5.48 us
    all_gather x1, waiting for transfers between devices, on_device(): lax.all_gather(jnp.concatenate([out_weight, dense_gate, dense_up, dense_d...  4.82 us
  transfers between devices with their start and end apart: 8, of which 4 were waited for; matrix products, arithmetic and copies ran while one was open for 3% of the time, Pallas kernels for 3%

profile of v3, /device:TPU:1, one launch (start us, length us, event | category | flops | bytes accessed | tf_op | source)
XLA Modules:
  0.0 221.4 jit_solution(16664396852144961483)
XLA Ops:
  7.3 1.7 pad_maximum_fusion.1
  9.0 0.8 constant_dynamic-update-slice_fusion.1
  9.8 0.8 constant_dynamic-update-slice_fusion
  10.7 4.4 %collective-permute-start.2 = (bf16[128,512]{1,0:T(8,128)(2,1)S(1)}, bf16[128,512]{1,0:T(8,128)(2,1)S(1)}, u32[]{:S(2)}, u32[]{:S(2)}) collective-permute-start(bf16[128,512]{1,0:T(8,128)(2,1)S(1)} %constant_dynamic-update-slice_fusion), channel_id=1, source_target_pairs={{0,32},{32,64},{64,96},{96,0},{1,33},{33,65},{65,97},{97,1},{2,34}... | collective-permute-start | bytes 393224 | tf_op jit(solution)/shard_map/ppermute | solution.py:276
  15.0 4.9 %collective-permute-start.1 = (bf16[128,512]{1,0:T(8,128)(2,1)S(1)}, bf16[128,512]{1,0:T(8,128)(2,1)S(1)}, u32[]{:S(2)}, u32[]{:S(2)}) collective-permute-start(bf16[128,512]{1,0:T(8,128)(2,1)S(1)} %constant_dynamic-update-slice_fusion), channel_id=1, source_target_pairs={{0,64},{32,96},{64,0},{96,32},{1,65},{33,97},{65,1},{97,33},{2,66}... | collective-permute-start | bytes 393224 | tf_op jit(solution)/shard_map/ppermute | solution.py:276
  19.9 2.6 %collective-permute-start = (bf16[128,512]{1,0:T(8,128)(2,1)S(1)}, bf16[128,512]{1,0:T(8,128)(2,1)S(1)}, u32[]{:S(2)}, u32[]{:S(2)}) collective-permute-start(bf16[128,512]{1,0:T(8,128)(2,1)S(1)} %constant_dynamic-update-slice_fusion), channel_id=1, source_target_pairs={{0,96},{32,0},{64,32},{96,64},{1,97},{33,1},{65,33},{97,65},{2,98}... | collective-permute-start | bytes 393224 | tf_op jit(solution)/shard_map/ppermute | solution.py:276
  22.6 1.1 fusion.10
  23.8 0.8 fusion.12
  24.6 0.2 reshape.70
  24.8 0.6 copy.83
  25.5 13.0 %all-to-all-start = ((bf16[4,16,128]{2,1,0:T(8,128)(2,1)}), bf16[4,16,128]{2,1,0:T(8,128)(2,1)S(1)}, u32[]{:S(2)}, u32[]{:S(2)}) async-start(bf16[4,16,128]{2,1,0:T(8,128)(2,1)} %bitcast.26), calls=%async_computation | async-start | bytes 32768 | tf_op jit(solution)/shard_map/all_to_all | solution.py:18
  38.6 0.1 eq.34
  38.8 0.1 reduce_window_sum.11
  38.9 0.1 maximum_maximum_fusion.maps_ref
  39.1 0.2 select_reduce_fusion
  39.3 0.1 reduce_sum.58
  39.5 0.2 slice_reduce_fusion.1
  39.7 3.7 %collective-permute-start.3 = (bf16[512,512]{1,0:T(8,128)(2,1)S(1)}, bf16[512,512]{1,0:T(8,128)(2,1)S(1)}, u32[]{:S(2)}, u32[]{:S(2)}) collective-permute-start(bf16[512,512]{1,0:T(8,128)(2,1)S(1)} %pad_maximum_fusion.mine_ref), channel_id=1, source_target_pairs={{0,16},{16,0},{1,17},{17,1},{2,18},{18,2},{3,19},{19,3},{4,20},{20... | collective-permute-start | bytes 1572872 | tf_op jit(solution)/shard_map/ppermute | solution.py:243
  43.5 6.5 %all-to-all-done = bf16[4,16,128]{2,1,0:T(8,128)(2,1)S(1)} async-done(((bf16[4,16,128]{2,1,0:T(8,128)(2,1)}), bf16[4,16,128]{2,1,0:T(8,128)(2,1)S(1)}, u32[]{:S(2)}, u32[]{:S(2)}) %all-to-all-start) | async-done | bytes 16416 | tf_op jit(solution)/shard_map/all_to_all | solution.py:18
  50.1 14.1 %all_to_all.45.rows_ref = bf16[16,64,128]{2,1,0:T(8,128)(2,1)S(1)} all-to-all(bf16[16,64,128]{2,1,0:T(8,128)(2,1)S(1)} %broadcast_in_dim.20), channel_id=1, replica_groups=mesh['far'=4,'near'=4,'core'=2,'tp'=16] {'tp'}, dimensions={0} | all-to-all | bytes 524288 | tf_op jit(solution)/shard_map/all_to_all | solution.py:18
  64.2 1.1 shard_map.220
  65.3 6.2 %all-to-all-start.2 = ((bf16[4,32,512]{2,1,0:T(8,128)(2,1)}), bf16[4,32,512]{2,1,0:T(8,128)(2,1)S(1)}, u32[]{:S(2)}, u32[]{:S(2)}) async-start(bf16[4,32,512]{2,1,0:T(8,128)(2,1)} %shard_map.220), calls=%async_computation.2 | async-start | bytes 262144 | tf_op jit(solution)/shard_map/all_to_all | solution.py:18
  71.5 15.7 %all-to-all-done.2 = bf16[4,32,512]{2,1,0:T(8,128)(2,1)S(1)} async-done(((bf16[4,32,512]{2,1,0:T(8,128)(2,1)}), bf16[4,32,512]{2,1,0:T(8,128)(2,1)S(1)}, u32[]{:S(2)}, u32[]{:S(2)}) %all-to-all-start.2) | async-done | bytes 131104 | tf_op jit(solution)/shard_map/all_to_all | solution.py:18
  87.3 0.1 convert_element_type.70
  87.4 0.1 fusion.3
  87.6 0.1 div.34
  87.7 0.2 fusion.7
  87.9 0.1 div.32
  88.0 0.6 fusion.15
  88.7 0.7 fusion.22
  89.3 4.8 %all-gather.3.cloned.1.call-done = bf16[20480,128]{1,0:T(8,128)(2,1)} async-done(((bf16[640,128]{1,0:T(8,128)(2,1)}), bf16[20480,128]{1,0:T(8,128)(2,1)}) %all-gather.3.cloned.1.call-update) | async-done | bytes 5242896 | tf_op jit(solution)/shard_map/all_gather | solution.py:244
  94.2 3.3 %shard_map.221 = bf16[16,32,256]{2,1,0:T(8,128)(2,1)} custom-call(bf16[32,256]{1,0:T(8,128)(2,1)} %get-tuple-element.22.rows_ref, bf16[32,640,128]{2,1,0:T(8,128)(2,1)} %bitcast.28), custom_call_target="tpu_custom_call" | custom-call | flops 67108864 | bytes 2097152 | tf_op jit(solution)/shard_map/pallas_call | solution.py:98
  97.5 15.7 %all_to_all.46 = bf16[16,32,256]{2,1,0:T(8,128)(2,1)S(1)} all-to-all(bf16[16,32,256]{2,1,0:T(8,128)(2,1)} %shard_map.221), channel_id=1, replica_groups=mesh['far'=4,'near'=4,'core'=2,'tp'=16] {'tp'}, dimensions={0} | all-to-all | bytes 524288 | tf_op jit(solution)/shard_map/all_to_all | solution.py:18
  113.2 0.1 convolution_convert_fusion
  113.4 0.7 reshape.74
  114.0 9.1 %all-to-all-start.4 = ((bf16[32,4,256]{2,1,0:T(4,128)(2,1)}), bf16[32,4,256]{2,1,0:T(4,128)(2,1)S(1)}, u32[]{:S(2)}, u32[]{:S(2)}) async-start(bf16[32,4,256]{2,1,0:T(4,128)(2,1)} %reshape.74), calls=%async_computation.4 | async-start | bytes 131072 | tf_op jit(solution)/shard_map/all_to_all | solution.py:18
  123.1 5.5 %shard_map.222 = (bf16[4096,256]{1,0:T(8,128)(2,1)}, bf16[128,4096]{1,0:T(8,128)(2,1)}, bf16[32,384,128]{2,1,0:T(8,128)(2,1)}) custom-call(bf16[4096,128]{1,0:T(8,128)(2,1)} %bitcast.31, bf16[4096,128]{1,0:T(8,128)(2,1)} %bitcast.32, bf16[128,4096]{1,0:T(8,128)(2,1)} %bitcast.33, bf16[32,640,128]{2,1,0:T(8,128)(2,1)} %bitcast.29), custom_call_target="tpu_custom_call" | custom-call | flops 40000000 | bytes 3145728 | tf_op jit(solution)/shard_map/pallas_call | solution.py:131
  128.6 7.5 %all-to-all-done.4 = bf16[32,4,256]{2,1,0:T(4,128)(2,1)S(1)} async-done(((bf16[32,4,256]{2,1,0:T(4,128)(2,1)}), bf16[32,4,256]{2,1,0:T(4,128)(2,1)S(1)}, u32[]{:S(2)}, u32[]{:S(2)}) %all-to-all-start.4) | async-done | bytes 65568 | tf_op jit(solution)/shard_map/all_to_all | solution.py:18
  136.1 0.1 broadcast_in_dim.22
  136.3 20.9 %all_to_all.47.pieces_ref = bf16[16,160,256]{2,1,0:T(8,128)(2,1)S(1)} all-to-all(bf16[16,160,256]{2,1,0:T(8,128)(2,1)S(1)} %broadcast_in_dim.22), channel_id=1, replica_groups=mesh['far'=4,'near'=4,'core'=2,'tp'=16] {'tp'}, dimensions={0} | all-to-all | bytes 2621440 | tf_op jit(solution)/shard_map/all_to_all | solution.py:18
  157.2 1.6 copy-done.2
  158.8 1.8 shard_map.223
  160.7 20.0 %all_to_all.48 = bf16[16,160,256]{2,1,0:T(8,128)(2,1)S(1)} all-to-all(bf16[16,160,256]{2,1,0:T(8,128)(2,1)S(1)} %get-tuple-element.34), channel_id=1, replica_groups=mesh['far'=4,'near'=4,'core'=2,'tp'=16] {'tp'}, dimensions={0} | all-to-all | bytes 2621440 | tf_op jit(solution)/shard_map/all_to_all | solution.py:18
  180.6 0.2 convert_reduce_fusion
  180.9 22.6 %all_to_all.49 = bf16[32,4,256]{2,1,0:T(4,128)(2,1)S(1)} all-to-all(bf16[32,4,256]{2,1,0:T(4,128)(2,1)S(1)} %reshape.77), channel_id=1, replica_groups=mesh['far'=4,'near'=4,'core'=2,'tp'=16] {'far','near','core'}, dimensions={0} | all-to-all | bytes 131072 | tf_op jit(solution)/shard_map/all_to_all | solution.py:18
  203.5 0.1 fusion.9
  203.6 10.2 %all_to_all.50 = bf16[16,32,256]{2,1,0:T(8,128)(2,1)S(1)} all-to-all(bf16[16,32,256]{2,1,0:T(8,128)(2,1)S(1)} %broadcast_in_dim.23), channel_id=1, replica_groups=mesh['far'=4,'near'=4,'core'=2,'tp'=16] {'tp'}, dimensions={0} | all-to-all | bytes 524288 | tf_op jit(solution)/shard_map/all_to_all | solution.py:18
  213.8 0.7 copy.77
  (61 shorter events, 0.9 us)
Async XLA Ops:
  7.2 80.2 %copy-start = (bf16[4,64,64]{2,1,0:T(8,128)(2,1)S(1)}, bf16[4,64,64]{2,1,0:T(8,128)(2,1)}, u32[]{:S(2)}) copy-start(bf16[4,64,64]{2,1,0:T(8,128)(2,1)} %param.29) | copy-start | bytes 98308
  7.2 16.6 %copy-start.5 = (bf16[32,4096]{1,0:T(8,128)(2,1)S(1)}, bf16[32,4096]{1,0:T(8,128)(2,1)}, u32[]{:S(2)}) copy-start(bf16[32,4096]{1,0:T(8,128)(2,1)} %param.21) | copy-start | bytes 786436
  7.2 31.3 %copy-start.10 = (s32[32,2]{0,1:T(2,128)S(1)}, s32[32,2]{0,1:T(2,128)}, u32[]{:S(2)}) copy-start(s32[32,2]{0,1:T(2,128)} %param.34) | copy-start | bytes 772
  7.2 31.5 %copy-start.9 = (bf16[4096]{0:T(1024)(128)(2,1)S(1)}, bf16[4096]{0:T(1024)(128)(2,1)}, u32[]{:S(2)}) copy-start(bf16[4096]{0:T(1024)(128)(2,1)} %param.41) | copy-start | bytes 24580
  7.2 31.7 %copy-start.6 = (bf16[4096,32]{0,1:T(8,128)(2,1)S(1)}, bf16[4096,32]{0,1:T(8,128)(2,1)}, u32[]{:S(2)}) copy-start(bf16[4096,32]{0,1:T(8,128)(2,1)} %param.33) | copy-start | bytes 786436
  7.2 86.9 %all-gather.3.cloned.1.call-start = ((), (), s32[]{:S(2)}) async-start(), calls=%async_computation.9 | async-start | bytes 5406720 | tf_op jit(solution)/shard_map/all_gather | solution.py:244
  10.7 29.0 %collective-permute-start.2 = (bf16[128,512]{1,0:T(8,128)(2,1)S(1)}, bf16[128,512]{1,0:T(8,128)(2,1)S(1)}, u32[]{:S(2)}, u32[]{:S(2)}) collective-permute-start(bf16[128,512]{1,0:T(8,128)(2,1)S(1)} %constant_dynamic-update-slice_fusion), channel_id=1, source_target_pairs={{0,32},{32,64},{64,96},{96,0},{1,33},{33,65},{65,97},{97,1},{2,34}... | collective-permute-start | bytes 393224 | tf_op jit(solution)/shard_map/ppermute | solution.py:276
  15.0 24.6 %collective-permute-start.1 = (bf16[128,512]{1,0:T(8,128)(2,1)S(1)}, bf16[128,512]{1,0:T(8,128)(2,1)S(1)}, u32[]{:S(2)}, u32[]{:S(2)}) collective-permute-start(bf16[128,512]{1,0:T(8,128)(2,1)S(1)} %constant_dynamic-update-slice_fusion), channel_id=1, source_target_pairs={{0,64},{32,96},{64,0},{96,32},{1,65},{33,97},{65,1},{97,33},{2,66}... | collective-permute-start | bytes 393224 | tf_op jit(solution)/shard_map/ppermute | solution.py:276
  19.9 19.7 %collective-permute-start = (bf16[128,512]{1,0:T(8,128)(2,1)S(1)}, bf16[128,512]{1,0:T(8,128)(2,1)S(1)}, u32[]{:S(2)}, u32[]{:S(2)}) collective-permute-start(bf16[128,512]{1,0:T(8,128)(2,1)S(1)} %constant_dynamic-update-slice_fusion), channel_id=1, source_target_pairs={{0,96},{32,0},{64,32},{96,64},{1,97},{33,1},{65,33},{97,65},{2,98}... | collective-permute-start | bytes 393224 | tf_op jit(solution)/shard_map/ppermute | solution.py:276
  25.5 24.6 %all-to-all-start = ((bf16[4,16,128]{2,1,0:T(8,128)(2,1)}), bf16[4,16,128]{2,1,0:T(8,128)(2,1)S(1)}, u32[]{:S(2)}, u32[]{:S(2)}) async-start(bf16[4,16,128]{2,1,0:T(8,128)(2,1)} %bitcast.26), calls=%async_computation | async-start | bytes 32768 | tf_op jit(solution)/shard_map/all_to_all | solution.py:18
  39.7 31.8 %copy-start.12 = (f32[256]{0:T(256)S(1)}, f32[256]{0:T(256)}, u32[]{:S(2)}) copy-start(f32[256]{0:T(256)} %param.30) | copy-start | bytes 3076
  39.7 24.4 %collective-permute-start.3 = (bf16[512,512]{1,0:T(8,128)(2,1)S(1)}, bf16[512,512]{1,0:T(8,128)(2,1)S(1)}, u32[]{:S(2)}, u32[]{:S(2)}) collective-permute-start(bf16[512,512]{1,0:T(8,128)(2,1)S(1)} %pad_maximum_fusion.mine_ref), channel_id=1, source_target_pairs={{0,16},{16,0},{1,17},{17,1},{2,18},{18,2},{3,19},{19,3},{4,20},{20... | collective-permute-start | bytes 1572872 | tf_op jit(solution)/shard_map/ppermute | solution.py:243
  50.0 37.2 %copy-start.7 = (bf16[32,3,256]{2,0,1:T(8,128)(2,1)S(1)}, bf16[32,3,256]{2,0,1:T(8,128)(2,1)}, u32[]{:S(2)}) copy-start(bf16[32,3,256]{2,0,1:T(8,128)(2,1)} %param.23) | copy-start | bytes 147460
  50.0 37.2 %copy-start.11 = (f32[4,256]{1,0:T(4,128)S(1)}, f32[4,256]{1,0:T(4,128)}, u32[]{:S(2)}) copy-start(f32[4,256]{1,0:T(4,128)} %param.27) | copy-start | bytes 12292
  64.2 23.6 %copy-start.13 = (bf16[4,64,64]{2,1,0:T(8,128)(2,1)S(1)}, bf16[4,64,64]{2,1,0:T(8,128)(2,1)}, u32[]{:S(2)}) copy-start(bf16[4,64,64]{2,1,0:T(8,128)(2,1)} %param.28) | copy-start | bytes 98308
  64.2 24.5 %copy-start.8 = (f32[32,256]{1,0:T(8,128)S(1)}, f32[32,256]{1,0:T(8,128)}, u32[]{:S(2)}) copy-start(f32[32,256]{1,0:T(8,128)} %param.22) | copy-start | bytes 98308
  65.3 21.9 %all-to-all-start.2 = ((bf16[4,32,512]{2,1,0:T(8,128)(2,1)}), bf16[4,32,512]{2,1,0:T(8,128)(2,1)S(1)}, u32[]{:S(2)}, u32[]{:S(2)}) async-start(bf16[4,32,512]{2,1,0:T(8,128)(2,1)} %shard_map.220), calls=%async_computation.2 | async-start | bytes 262144 | tf_op jit(solution)/shard_map/all_to_all | solution.py:18
  114.0 22.1 %all-to-all-start.4 = ((bf16[32,4,256]{2,1,0:T(4,128)(2,1)}), bf16[32,4,256]{2,1,0:T(4,128)(2,1)S(1)}, u32[]{:S(2)}, u32[]{:S(2)}) async-start(bf16[32,4,256]{2,1,0:T(4,128)(2,1)} %reshape.74), calls=%async_computation.4 | async-start | bytes 131072 | tf_op jit(solution)/shard_map/all_to_all | solution.py:18
  136.1 21.1 %copy-start.3 = (bf16[128,4096]{1,0:T(8,128)(2,1)S(1)}, bf16[128,4096]{1,0:T(8,128)(2,1)}, u32[]{:S(2)}) copy-start(bf16[128,4096]{1,0:T(8,128)(2,1)} %get-tuple-element.29.down_ref) | copy-start | bytes 3145732
  136.1 21.1 %copy-start.1 = (bf16[32,384,128]{2,1,0:T(8,128)(2,1)S(1)}, bf16[32,384,128]{2,1,0:T(8,128)(2,1)}, u32[]{:S(2)}) copy-start(bf16[32,384,128]{2,1,0:T(8,128)(2,1)} %get-tuple-element.30.dense_ref) | copy-start | bytes 9437188
  136.3 21.0 %copy-start.4 = (f32[4096]{0:T(1024)S(1)}, f32[4096]{0:T(1024)}, u32[]{:S(2)}) copy-start(f32[4096]{0:T(1024)} %param.32) | copy-start | bytes 49156
  157.2 1.6 copy-start.2
Sparse Core Ops, SparseCore 0:
  10.7 83.3 all-gather.2

commit v4 on v3

--- a/solution.py
+++ b/solution.py
@@ -69,145 +69,146 @@
 ROOMY = 60 * 1024 * 1024
 
 
-def output_kernel(rows_ref, whole_hbm, out_ref, weight_ref, sems):
+def output_kernel(rows_hbm, whole_hbm, out_hbm, rows_ref, weight_ref, out_ref, row_sem, in_sems, out_sems):
     channels = rows_ref.shape[1]
     chips = out_ref.shape[0]
-    steps = 4
-    owners = 2 * chips // steps
+    steps = in_sems.shape[0]
+    each = chips // steps
+    owners = 2 * each
+    row_copy = pltpu.make_async_copy(rows_hbm, rows_ref, row_sem)
+    row_copy.start()
     copies = [
         pltpu.make_async_copy(
             whole_hbm.at[pl.ds(i * owners, owners), pl.ds(0, channels)],
             weight_ref.at[pl.ds(i * owners, owners)],
-            sems.at[i],
+            in_sems.at[i],
         )
         for i in range(steps)
     ]
     for copy in copies:
         copy.start()
+    row_copy.wait()
     rows = rows_ref[...]
-    for z in range(chips):
-        if z % (chips // steps) == 0:
-            copies[z // (chips // steps)].wait()
-        weight = jnp.concatenate([weight_ref[2 * z], weight_ref[2 * z + 1]], axis=1)
-        out_ref[z] = dot(rows, weight).astype(jnp.bfloat16)
+    results = []
+    for i in range(steps):
+        copies[i].wait()
+        for z in range(i * each, (i + 1) * each):
+            weight = jnp.concatenate([weight_ref[2 * z], weight_ref[2 * z + 1]], axis=1)
+            out_ref[z] = dot(rows, weight).astype(jnp.bfloat16)
+        result = pltpu.make_async_copy(
+            out_ref.at[pl.ds(i * each, each)], out_hbm.at[pl.ds(i * each, each)], out_sems.at[i]
+        )
+        result.start()
+        results.append(result)
+    for result in results:
+        result.wait()
 
 
 def output_product(rows, whole):
     owners, _, lanes = whole.shape
     channels = rows.shape[1]
+    out = jax.ShapeDtypeStruct((owners // 2, rows.shape[0], 2 * lanes), jnp.bfloat16)
+    anywhere = pl.BlockSpec(memory_space=pl.ANY)
+    steps = 4
     return pl.pallas_call(
         output_kernel,
-        out_shape=jax.ShapeDtypeStruct((owners // 2, rows.shape[0], 2 * lanes), jnp.bfloat16),
-        in_specs=[vmem(), pl.BlockSpec(memory_space=pl.ANY)],
-        out_specs=vmem(),
-        scratch_shapes=[pltpu.VMEM((owners, channels, lanes), whole.dtype), pltpu.SemaphoreType.DMA((4,))],
+        out_shape=out,
+        in_specs=[anywhere, anywhere],
+        out_specs=anywhere,
+        scratch_shapes=[
+            pltpu.VMEM(rows.shape, rows.dtype),
+            pltpu.VMEM((owners, channels, lanes), whole.dtype),
+            pltpu.VMEM(out.shape, out.dtype),
+            pltpu.SemaphoreType.DMA,
+            pltpu.SemaphoreType.DMA((steps,)),
+            pltpu.SemaphoreType.DMA((steps,)),
+        ],
         compiler_params=pltpu.CompilerParams(vmem_limit_bytes=ROOMY),
         cost_estimate=pl.CostEstimate(flops=2 * rows.size * owners * lanes, bytes_accessed=2 * owners * channels * lanes, transcendentals=0),
     )(rows, whole)
 
 
-def fetch_kernel(gate_hbm, up_hbm, down_hbm, whole_hbm, both_ref, down_ref, dense_ref, sems):
-    half = gate_hbm.shape[1]
-    owners, rows, _ = dense_ref.shape
+def experts_kernel(pieces_ref, gain_ref, maps_ref, facts_ref, gate_hbm, up_hbm, down_hbm, whole_hbm, out_ref, both_ref, down_ref, dense_ref, rows_ref, sems):
+    chips, slots, share = pieces_ref.shape
+    depth = share // 2
+    owners, dense_rows, _ = dense_ref.shape
     copies = [
         pltpu.make_async_copy(source, target, sems.at[i])
         for i, (source, target) in enumerate(
             (
-                (gate_hbm, both_ref.at[:, pl.ds(0, half)]),
-                (up_hbm, both_ref.at[:, pl.ds(half, half)]),
-                (whole_hbm.at[pl.ds(0, owners), pl.ds(whole_hbm.shape[1] - rows, rows)], dense_ref),
+                (gate_hbm, both_ref.at[:, pl.ds(0, depth)]),
+                (up_hbm, both_ref.at[:, pl.ds(depth, depth)]),
+                (whole_hbm.at[pl.ds(0, owners), pl.ds(whole_hbm.shape[1] - dense_rows, dense_rows)], dense_ref),
                 (down_hbm, down_ref),
             )
         )
     ]
     for copy in copies:
         copy.start()
-    for copy in copies:
-        copy.wait()
-
-
-def fetch_weights(gate, up, down, whole, dense_rows):
-    owners, _, lanes = whole.shape
-    return pl.pallas_call(
-        fetch_kernel,
-        out_shape=(
-            jax.ShapeDtypeStruct((gate.shape[0], 2 * gate.shape[1]), gate.dtype),
-            jax.ShapeDtypeStruct(down.shape, down.dtype),
-            jax.ShapeDtypeStruct((owners, dense_rows, lanes), whole.dtype),
-        ),
-        in_specs=[pl.BlockSpec(memory_space=pl.ANY)] * 4,
-        out_specs=(vmem(),) * 3,
-        scratch_shapes=[pltpu.SemaphoreType.DMA((4,))],
-        compiler_params=pltpu.CompilerParams(vmem_limit_bytes=54 * 1024 * 1024),
-        cost_estimate=pl.CostEstimate(flops=40_000_000, bytes_accessed=6 * gate.size, transcendentals=0),
-    )(gate, up, down, whole)
-
-
-def experts_kernel(pieces_ref, gain_ref, both_ref, down_ref, dense_ref, maps_ref, picks_ref, places_ref, out_ref, combine_ref, branch_ref):
-    chips, count, share = pieces_ref.shape
-    depth = share // 2
-    slots = down_ref.shape[0]
-    rows_own = count - slots
-    squares = jnp.zeros((count, share), jnp.float32)
+    squares = jnp.zeros((slots, share), jnp.float32)
     for z in range(chips):
         values = pieces_ref[z].astype(jnp.float32)
         squares = squares + values * values
     mean = jnp.sum(squares, axis=1, keepdims=True) / (chips * share)
     inverse = lax.rsqrt(mean + epsilon)
+    copies[0].wait()
+    copies[1].wait()
     routed = jnp.zeros((slots, share), jnp.float32)
-    dense = jnp.zeros((rows_own, share), jnp.float32)
-    logits = jnp.zeros((rows_own, maps_ref.shape[0]), jnp.float32)
+    dense = jnp.zeros((slots, share), jnp.float32)
+    logits = jnp.zeros((slots, maps_ref.shape[0]), jnp.float32)
     for z in range(chips):
         at = pl.ds(z * share, share)
         rows = (pieces_ref[z].astype(jnp.float32) * inverse * gain_ref[:, at]).astype(jnp.bfloat16)
-        routed = routed + dot(rows[:slots], both_ref[at, :])
+        rows_ref[z] = rows
+        routed = routed + dot(rows, both_ref[at, :])
+        logits = logits + lax.dot_general(
+            rows, maps_ref[:, at], (((1,), (1,)), ((), ())), preferred_element_type=jnp.float32
+        )
+    copies[2].wait()
+    for z in range(chips):
         weights = [
             jnp.concatenate([dense_ref[2 * z + c, i * depth : (i + 1) * depth] for c in range(2)], axis=0)
             for i in range(2)
         ]
-        dense = dense + dot(rows[slots:], jnp.concatenate(weights, axis=1))
-        logits = logits + lax.dot_general(
-            rows[slots:], maps_ref[:, at], (((1,), (1,)), ((), ())), preferred_element_type=jnp.float32
-        )
+        dense = dense + dot(rows_ref[z], jnp.concatenate(weights, axis=1))
+    copies[3].wait()
     half = share // 2
     routed_act = (jax.nn.silu(routed[:, :half]) * routed[:, half:]).astype(jnp.bfloat16)
     dense_act = (jax.nn.silu(dense[:, :half]) * dense[:, half:]).astype(jnp.bfloat16)
-    for z in range(chips):
-        out_ref[z, :slots, :] = dot(routed_act, down_ref[:, pl.ds(z * share, share)]).astype(jnp.bfloat16)
-        weight = jnp.concatenate([dense_ref[2 * z + c, 2 * depth :] for c in range(2)], axis=1)
-        out_ref[z, slots:, :] = dot(dense_act, weight).astype(jnp.bfloat16)
-
-    experts = maps_ref.shape[0] - 8
-    column = lax.broadcasted_iota(jnp.int32, logits.shape, 1)
+
+    facts = facts_ref[...].astype(jnp.float32)
+    column = lax.broadcasted_iota(jnp.int32, logits.shape, 1).astype(jnp.float32)
 
     def of_column(index):
         return jnp.sum(jnp.where(column == index, logits, 0.0), axis=1, keepdims=True)
 
-    picked = [of_column(picks_ref[:, k : k + 1]) for k in range(TOP_K)]
-    place = lax.broadcasted_iota(jnp.int32, (rows_own, combine_ref.shape[1]), 1)
-    total = jnp.zeros((rows_own, combine_ref.shape[1]), jnp.float32)
-    for k in range(TOP_K):
-        weight = jax.nn.sigmoid(picked[k] - picked[1 - k]).astype(jnp.bfloat16).astype(jnp.float32)
-        total = total + jnp.where(place == places_ref[:, k : k + 1], weight, 0.0)
-    combine_ref[...] = total.astype(jnp.bfloat16)
-    branch_ref[...] = jnp.broadcast_to(jax.nn.sigmoid(of_column(experts)), branch_ref.shape)
-
-
-def experts_product(pieces, gain, both, down, dense, maps, picks, places):
-    _, count, share = pieces.shape
-    own_rows = picks.shape[0]
+    expert_weight = jax.nn.sigmoid(of_column(facts[:, 0:1]) - of_column(facts[:, 1:2]))
+    expert_weight = expert_weight.astype(jnp.bfloat16).astype(jnp.float32)
+    branch_weight = jax.nn.sigmoid(of_column(float(maps_ref.shape[0] - 8))) * facts[:, 2:3]
+    for z in range(chips):
+        weight = jnp.concatenate([dense_ref[2 * z + c, 2 * depth :] for c in range(2)], axis=1)
+        part = expert_weight * dot(routed_act, down_ref[:, pl.ds(z * share, share)])
+        out_ref[z] = (part + branch_weight * dot(dense_act, weight)).astype(jnp.bfloat16)
+
+
+def experts_product(pieces, gain, maps, facts, gate, up, down, whole, dense_rows):
+    owners, _, lanes = whole.shape
+    anywhere = pl.BlockSpec(memory_space=pl.ANY)
     return pl.pallas_call(
         experts_kernel,
-        out_shape=(
-            jax.ShapeDtypeStruct(pieces.shape, jnp.bfloat16),
-            jax.ShapeDtypeStruct((own_rows, count - own_rows), jnp.bfloat16),
-            jax.ShapeDtypeStruct((own_rows, share), jnp.float32),
-        ),
-        in_specs=[vmem()] * 8,
-        out_specs=(vmem(),) * 3,
-        compiler_params=pltpu.CompilerParams(vmem_limit_bytes=16 * 1024 * 1024),
-        cost_estimate=pl.CostEstimate(flops=3 * count * both.size, bytes_accessed=6 * both.size, transcendentals=0),
-    )(pieces, gain, both, down, dense, maps, picks, places)
+        out_shape=jax.ShapeDtypeStruct(pieces.shape, jnp.bfloat16),
+        in_specs=[*([vmem()] * 4), *([anywhere] * 4)],
+        out_specs=vmem(),
+        scratch_shapes=[
+            pltpu.VMEM((gate.shape[0], 2 * gate.shape[1]), gate.dtype),
+            pltpu.VMEM(down.shape, down.dtype),
+            pltpu.VMEM((owners, dense_rows, lanes), whole.dtype),
+            pltpu.VMEM(pieces.shape, pieces.dtype),
+            pltpu.SemaphoreType.DMA((4,)),
+        ],
+        compiler_params=pltpu.CompilerParams(vmem_limit_bytes=ROOMY),
+        cost_estimate=pl.CostEstimate(flops=12 * pieces.shape[1] * gate.size, bytes_accessed=12 * gate.size, transcendentals=0),
+    )(pieces, gain, maps, facts, gate, up, down, whole)
 
 
 def on_device(
@@ -235,6 +236,7 @@
 ):
     batch_rows, width = tokens.shape
     depth, channels = in_weight.shape
+    lanes = out_weight.shape[1]
     columns = lax.axis_size("tp")
     share = width // columns
     far, near = lax.axis_size("far"), lax.axis_size("near")
@@ -262,13 +264,26 @@
     slot_of = (flat_ids * capacity + rank).reshape(batch_rows, TOP_K)
     slots = experts * capacity
     slot_rows = lax.broadcasted_iota(jnp.int32, (slots, batch_rows), 0)
-    dispatch = sum((slot_rows == slot_of[None, :, pick]).astype(jnp.bfloat16) for pick in range(TOP_K))
+    picks = [(slot_rows == slot_of[None, :, pick]).astype(jnp.bfloat16) for pick in range(TOP_K)]
+    dispatch = picks[0] + picks[1]
+    lane = lax.broadcasted_iota(jnp.int32, (batch_rows, lanes), 1)
+    facts = sum(
+        dot(
+            picks[k],
+            jnp.where(
+                lane == 0,
+                routes[:, k : k + 1],
+                jnp.where(lane == 1, routes[:, 1 - k : 2 - k], jnp.where(lane == 2, 1 - k, 0)),
+            ).astype(jnp.bfloat16),
+        )
+        for k in range(TOP_K)
+    ).astype(jnp.bfloat16)
     maps = jnp.concatenate(
         [router_weight.T, branch_gate.reshape(1, width), jnp.zeros((7, width), jnp.bfloat16)], axis=0
     )
     own_tokens = lax.dynamic_slice_in_dim(tokens, column * share, share, 1)
-    came, dispatch, slot_of, maps, own_tokens = lax.optimization_barrier(
-        (came, dispatch, slot_of, maps, own_tokens)
+    came, dispatch, facts, maps, own_tokens = lax.optimization_barrier(
+        (came, dispatch, facts, maps, own_tokens)
     )
 
     block_rows = copies_to_all(came, "tp")
@@ -303,22 +318,25 @@
     mixed_share = exchange(mixer_part, "tp").astype(jnp.float32).sum(axis=0)
     resid_share = (own_tokens.astype(jnp.float32) + mixed_share).astype(jnp.bfloat16)
 
-    outgoing = dot(dispatch, resid_share).astype(jnp.bfloat16)
-    arrived = exchange(outgoing.reshape(experts, capacity, share), EP).reshape(slots, share)
-    fetched = fetch_weights(expert_gate[0], expert_up[0], expert_down[0], whole, 3 * depth)
-    arrived, fetched = lax.optimization_barrier((arrived, fetched))
-    shares = jnp.concatenate([arrived, resid_share], axis=0)
-    parts_cut, combine, branch_weight = experts_product(
-        copies_to_all(shares, "tp"), ffn_gain.reshape(1, width), *fetched, maps, routes, slot_of
+    outgoing = jnp.concatenate([dot(dispatch, resid_share).astype(jnp.bfloat16), facts], axis=1)
+    arrived = exchange(outgoing.reshape(experts, capacity, -1), EP).reshape(slots, -1)
+    arrived_share, arrived_facts = lax.optimization_barrier((arrived[:, :share], arrived[:, share:]))
+    pieces = copies_to_all(arrived_share, "tp")
+    parts_cut = experts_product(
+        pieces,
+        ffn_gain.reshape(1, width),
+        maps,
+        arrived_facts,
+        expert_gate[0],
+        expert_up[0],
+        expert_down[0],
+        whole,
+        3 * depth,
     )
-    sums = exchange(parts_cut, "tp").astype(jnp.float32).sum(axis=0)
-    total, dense_share = sums[:slots].astype(jnp.bfloat16), sums[slots:]
-
+    total = exchange(parts_cut, "tp").astype(jnp.float32).sum(axis=0).astype(jnp.bfloat16)
     returned = exchange(total.reshape(experts, capacity, share), EP)
-    moe = dot(combine, returned.reshape(slots, share))
-    out_share = (
-        resid_share.astype(jnp.float32) + moe + branch_weight * dense_share
-    ).astype(jnp.bfloat16)
+    branches = dot(dispatch.T, returned.reshape(slots, share))
+    out_share = (resid_share.astype(jnp.float32) + branches).astype(jnp.bfloat16)
     layer_out = features_joined(copies_to_all(out_share, "tp"))
     return (layer_out, new_state, new_conv_state)
 

time: 223 us -> 221 us (level)
  waiting for transfers between devices: 34.6 us -> 15.2 us
  blocking collectives: 103 us -> 122 us
  starting transfers between devices: 43.9 us -> 40.2 us
  other arithmetic: 5.74 us -> 8.26 us
    all_to_all x6 -> x7, blocking collectives: 103 us -> 122 us  [exchange(): return lax.all_to_all(pieces, axis, split_axis=0, concat_axis=0, tiled=True)]
    all_to_all x3 -> x2, waiting for transfers between devices: 29.8 us -> 15.2 us  [exchange(): return lax.all_to_all(pieces, axis, split_axis=0, concat_axis=0, tiled=True)]
    all_gather x1, waiting for transfers between devices: 4.82 us -> 0.01 us  [on_device(): lax.all_gather(jnp.concatenate([out_weight, dense_gate, dense_up, dense_d...]
    all_to_all x3 -> x2, starting transfers between devices: 28.2 us -> 24.5 us  [exchange(): return lax.all_to_all(pieces, axis, split_axis=0, concat_axis=0, tiled=True)]
    pallas_call x3 -> x2, Pallas kernels: 10.6 us -> 9.26 us  [the longest x1 6.56 us: experts_product(): pl.pallas_call(experts_kernel, out_shape=jax.ShapeDtypeStruct(pieces.shap...]
  transfers between devices with their start and end apart: 8 -> 7, of which waited for: 4 -> 2; matrix products, arithmetic and copies ran while one was open for 3% -> 6% of each run, Pallas kernels for 3% -> 1%
where the time goes in v4:
time: 221 us; the launch traced here: 220 us
  blocking collectives  122 us (55%)
  starting transfers between devices  40.2 us (18%)
  waiting for transfers between devices  15.2 us (7%)
  between operations  14.4 us (7%)
  Pallas kernels  10.4 us (5%)
  other arithmetic  8.26 us (4%)
  local copies, waits for them, and re-layouts  7.87 us (4%)
    all_to_all x7, blocking collectives, exchange(): return lax.all_to_all(pieces, axis, split_axis=0, concat_axis=0, tiled=True)  122 us
    all_to_all x2, starting transfers between devices, exchange(): return lax.all_to_all(pieces, axis, split_axis=0, concat_axis=0, tiled=True)  24.5 us
    all_to_all x2, waiting for transfers between devices, exchange(): return lax.all_to_all(pieces, axis, split_axis=0, concat_axis=0, tiled=True)  15.2 us
    ppermute x3, starting transfers between devices, on_device(): lax.ppermute(both_weights, 'near', [(i, (i - k) % near) for i in range(ne...  11.9 us
    pallas_call x1, Pallas kernels, experts_product(): pl.pallas_call(experts_kernel, out_shape=jax.ShapeDtypeStruct(pieces.shap...  6.56 us
  transfers between devices with their start and end apart: 7, of which 2 were waited for; matrix products, arithmetic and copies ran while one was open for 6% of the time, Pallas kernels for 1%

profile of v4, /device:TPU:1, one launch (start us, length us, event | category | flops | bytes accessed | tf_op | source)
XLA Modules:
  0.0 219.6 jit_solution(2565368126532504987)
XLA Ops:
  7.3 1.6 pad_maximum_fusion.1
  8.9 0.8 constant_dynamic-update-slice_fusion.1
  9.8 0.8 constant_dynamic-update-slice_fusion
  10.6 4.4 %collective-permute-start.2 = (bf16[128,512]{1,0:T(8,128)(2,1)S(1)}, bf16[128,512]{1,0:T(8,128)(2,1)S(1)}, u32[]{:S(2)}, u32[]{:S(2)}) collective-permute-start(bf16[128,512]{1,0:T(8,128)(2,1)S(1)} %constant_dynamic-update-slice_fusion), channel_id=1, source_target_pairs={{0,32},{32,64},{64,96},{96,0},{1,33},{33,65},{65,97},{97,1},{2,34}... | collective-permute-start | bytes 393224 | tf_op jit(solution)/shard_map/ppermute | solution.py:291
  15.0 4.9 %collective-permute-start.1 = (bf16[128,512]{1,0:T(8,128)(2,1)S(1)}, bf16[128,512]{1,0:T(8,128)(2,1)S(1)}, u32[]{:S(2)}, u32[]{:S(2)}) collective-permute-start(bf16[128,512]{1,0:T(8,128)(2,1)S(1)} %constant_dynamic-update-slice_fusion), channel_id=1, source_target_pairs={{0,64},{32,96},{64,0},{96,32},{1,65},{33,97},{65,1},{97,33},{2,66}... | collective-permute-start | bytes 393224 | tf_op jit(solution)/shard_map/ppermute | solution.py:291
  19.9 2.6 %collective-permute-start = (bf16[128,512]{1,0:T(8,128)(2,1)S(1)}, bf16[128,512]{1,0:T(8,128)(2,1)S(1)}, u32[]{:S(2)}, u32[]{:S(2)}) collective-permute-start(bf16[128,512]{1,0:T(8,128)(2,1)S(1)} %constant_dynamic-update-slice_fusion), channel_id=1, source_target_pairs={{0,96},{32,0},{64,32},{96,64},{1,97},{33,1},{65,33},{97,65},{2,98}... | collective-permute-start | bytes 393224 | tf_op jit(solution)/shard_map/ppermute | solution.py:291
  22.6 1.1 fusion.10
  23.7 1.1 fusion.12
  24.8 0.2 reshape.70
  25.0 0.6 copy.77
  25.6 13.0 %all-to-all-start = ((bf16[4,16,128]{2,1,0:T(8,128)(2,1)}), bf16[4,16,128]{2,1,0:T(8,128)(2,1)S(1)}, u32[]{:S(2)}, u32[]{:S(2)}) async-start(bf16[4,16,128]{2,1,0:T(8,128)(2,1)} %bitcast.33), calls=%async_computation | async-start | bytes 32768 | tf_op jit(solution)/shard_map/all_to_all | solution.py:18
  38.6 0.7 reshape.73
  39.4 0.8 copy.64
  40.1 0.1 eq.53
  40.3 0.1 reduce_window_sum.11
  40.4 0.2 select_reduce_fusion
  40.6 0.1 reduce_sum.61
  40.9 0.7 multiply_add_fusion.1
  41.6 0.8 slice_bitcast_fusion.2
  42.3 0.2 fusion.14
  42.5 1.8 maximum_maximum_fusion.maps_ref
  44.3 0.2 fusion.8
  44.6 3.7 %collective-permute-start.3 = (bf16[512,512]{1,0:T(8,128)(2,1)S(1)}, bf16[512,512]{1,0:T(8,128)(2,1)S(1)}, u32[]{:S(2)}, u32[]{:S(2)}) collective-permute-start(bf16[512,512]{1,0:T(8,128)(2,1)S(1)} %pad_maximum_fusion.mine_ref), channel_id=1, source_target_pairs={{0,16},{16,0},{1,17},{17,1},{2,18},{18,2},{3,19},{19,3},{4,20},{20... | collective-permute-start | bytes 1572872 | tf_op jit(solution)/shard_map/ppermute | solution.py:245
  48.3 0.7 constant_dynamic-slice_fusion
  49.1 1.3 all-to-all-done
  50.4 14.0 %all_to_all.45.rows_ref = bf16[16,64,128]{2,1,0:T(8,128)(2,1)S(1)} all-to-all(bf16[16,64,128]{2,1,0:T(8,128)(2,1)S(1)} %broadcast_in_dim.56), channel_id=1, replica_groups=mesh['far'=4,'near'=4,'core'=2,'tp'=16] {'tp'}, dimensions={0} | all-to-all | bytes 524288 | tf_op jit(solution)/shard_map/all_to_all | solution.py:18
  64.4 1.1 shard_map.220
  65.5 11.5 %all-to-all-start.2 = ((bf16[4,32,512]{2,1,0:T(8,128)(2,1)}), bf16[4,32,512]{2,1,0:T(8,128)(2,1)S(1)}, u32[]{:S(2)}, u32[]{:S(2)}) async-start(bf16[4,32,512]{2,1,0:T(8,128)(2,1)} %shard_map.220), calls=%async_computation.2 | async-start | bytes 262144 | tf_op jit(solution)/shard_map/all_to_all | solution.py:18
  77.0 13.9 %all-to-all-done.2 = bf16[4,32,512]{2,1,0:T(8,128)(2,1)S(1)} async-done(((bf16[4,32,512]{2,1,0:T(8,128)(2,1)}), bf16[4,32,512]{2,1,0:T(8,128)(2,1)S(1)}, u32[]{:S(2)}, u32[]{:S(2)}) %all-to-all-start.2) | async-done | bytes 131104 | tf_op jit(solution)/shard_map/all_to_all | solution.py:18
  91.1 0.1 fusion.3
  91.3 0.1 div.34
  91.4 0.2 fusion.7
  91.7 0.1 div.32
  91.8 0.6 fusion.16
  92.4 0.7 fusion.23
  93.1 2.7 %shard_map.221 = bf16[16,32,256]{2,1,0:T(8,128)(2,1)} custom-call(bf16[32,256]{1,0:T(8,128)(2,1)} %get-tuple-element.14.rows_hbm, bf16[32,640,128]{2,1,0:T(8,128)(2,1)} %bitcast.34), custom_call_target="tpu_custom_call" | custom-call | flops 67108864 | bytes 2097152 | tf_op jit(solution)/shard_map/pallas_call | solution.py:113
  95.8 16.9 %all_to_all.46 = bf16[16,32,256]{2,1,0:T(8,128)(2,1)S(1)} all-to-all(bf16[16,32,256]{2,1,0:T(8,128)(2,1)} %shard_map.221), channel_id=1, replica_groups=mesh['far'=4,'near'=4,'core'=2,'tp'=16] {'tp'}, dimensions={0} | all-to-all | bytes 524288 | tf_op jit(solution)/shard_map/all_to_all | solution.py:18
  112.7 0.1 convolution_convert_fusion
  112.9 23.9 %all_to_all.47 = bf16[32,4,384]{2,1,0:T(4,128)(2,1)S(1)} all-to-all(bf16[32,4,384]{2,1,0:T(4,128)(2,1)S(1)} %reshape.74), channel_id=1, replica_groups=mesh['far'=4,'near'=4,'core'=2,'tp'=16] {'far','near','core'}, dimensions={0} | all-to-all | bytes 196608 | tf_op jit(solution)/shard_map/all_to_all | solution.py:18
  136.8 0.6 slice.45.facts_ref
  137.5 19.3 %all_to_all.48.pieces_ref = bf16[16,128,256]{2,1,0:T(8,128)(2,1)} all-to-all(bf16[16,128,256]{2,1,0:T(8,128)(2,1)S(1)} %broadcast_in_dim.58), channel_id=1, replica_groups=mesh['far'=4,'near'=4,'core'=2,'tp'=16] {'tp'}, dimensions={0} | all-to-all | bytes 2097152 | tf_op jit(solution)/shard_map/all_to_all | solution.py:18
  156.8 6.6 %shard_map.222 = bf16[16,128,256]{2,1,0:T(8,128)(2,1)} custom-call(bf16[16,128,256]{2,1,0:T(8,128)(2,1)} %all_to_all.48.pieces_ref, f32[1,4096]{1,0:T(1,128)} %bitcast.43, bf16[40,4096]{1,0:T(8,128)(2,1)} %maximum_maximum_fusion.maps_ref, bf16[128,128]{1,0:T(8,128)(2,1)} %slice.45.facts_ref, bf16[4096,128]{1,0:T(8,128)(2,1)} %bitcast.37, ...), custom_call_target="tpu_custom_call" | custom-call | flops 805306368 | bytes 6291456 | tf_op jit(solution)/shard_map/pallas_call | solution.py:197
  163.4 19.0 %all_to_all.49 = bf16[16,128,256]{2,1,0:T(8,128)(2,1)S(1)} all-to-all(bf16[16,128,256]{2,1,0:T(8,128)(2,1)} %shard_map.222), channel_id=1, replica_groups=mesh['far'=4,'near'=4,'core'=2,'tp'=16] {'tp'}, dimensions={0} | all-to-all | bytes 2097152 | tf_op jit(solution)/shard_map/all_to_all | solution.py:18
  182.3 0.1 reduce_sum.65
  182.5 19.1 %all_to_all.50 = bf16[32,4,256]{2,1,0:T(4,128)(2,1)S(1)} all-to-all(bf16[32,4,256]{2,1,0:T(4,128)(2,1)S(1)} %reshape.77), channel_id=1, replica_groups=mesh['far'=4,'near'=4,'core'=2,'tp'=16] {'far','near','core'}, dimensions={0} | all-to-all | bytes 131072 | tf_op jit(solution)/shard_map/all_to_all | solution.py:18
  201.6 0.2 fusion.9
  201.8 10.2 %all_to_all.51 = bf16[16,32,256]{2,1,0:T(8,128)(2,1)S(1)} all-to-all(bf16[16,32,256]{2,1,0:T(8,128)(2,1)S(1)} %broadcast_in_dim.59), channel_id=1, replica_groups=mesh['far'=4,'near'=4,'core'=2,'tp'=16] {'tp'}, dimensions={0} | all-to-all | bytes 524288 | tf_op jit(solution)/shard_map/all_to_all | solution.py:18
  212.1 0.7 copy.71
  (46 shorter events, 1.0 us)
Async XLA Ops:
  7.2 84.0 %copy-start = (bf16[4,64,64]{2,1,0:T(8,128)(2,1)S(1)}, bf16[4,64,64]{2,1,0:T(8,128)(2,1)}, u32[]{:S(2)}) copy-start(bf16[4,64,64]{2,1,0:T(8,128)(2,1)} %param.29) | copy-start | bytes 98308
  7.2 69.8 %copy-start.4 = (f32[256]{0:T(256)S(1)}, f32[256]{0:T(256)}, u32[]{:S(2)}) copy-start(f32[256]{0:T(256)} %param.30) | copy-start | bytes 3076
  7.2 83.8 %copy-start.1 = (bf16[32,3,256]{2,0,1:T(8,128)(2,1)S(1)}, bf16[32,3,256]{2,0,1:T(8,128)(2,1)}, u32[]{:S(2)}) copy-start(bf16[32,3,256]{2,0,1:T(8,128)(2,1)} %param.23) | copy-start | bytes 147460
  7.2 83.8 %copy-start.3 = (f32[4,256]{1,0:T(4,128)S(1)}, f32[4,256]{1,0:T(4,128)}, u32[]{:S(2)}) copy-start(f32[4,256]{1,0:T(4,128)} %param.27) | copy-start | bytes 12292
  7.2 84.2 %copy-start.5 = (bf16[4,64,64]{2,1,0:T(8,128)(2,1)S(1)}, bf16[4,64,64]{2,1,0:T(8,128)(2,1)}, u32[]{:S(2)}) copy-start(bf16[4,64,64]{2,1,0:T(8,128)(2,1)} %param.28) | copy-start | bytes 98308
  7.2 85.2 %copy-start.2 = (f32[32,256]{1,0:T(8,128)S(1)}, f32[32,256]{1,0:T(8,128)}, u32[]{:S(2)}) copy-start(f32[32,256]{1,0:T(8,128)} %param.22) | copy-start | bytes 98308
  7.2 85.8 %all-gather.3.cloned.1.call-start = ((), (), s32[]{:S(2)}) async-start(), calls=%async_computation.9 | async-start | bytes 5406720 | tf_op jit(solution)/shard_map/all_gather | solution.py:246
  10.6 33.9 %collective-permute-start.2 = (bf16[128,512]{1,0:T(8,128)(2,1)S(1)}, bf16[128,512]{1,0:T(8,128)(2,1)S(1)}, u32[]{:S(2)}, u32[]{:S(2)}) collective-permute-start(bf16[128,512]{1,0:T(8,128)(2,1)S(1)} %constant_dynamic-update-slice_fusion), channel_id=1, source_target_pairs={{0,32},{32,64},{64,96},{96,0},{1,33},{33,65},{65,97},{97,1},{2,34}... | collective-permute-start | bytes 393224 | tf_op jit(solution)/shard_map/ppermute | solution.py:291
  15.0 29.6 %collective-permute-start.1 = (bf16[128,512]{1,0:T(8,128)(2,1)S(1)}, bf16[128,512]{1,0:T(8,128)(2,1)S(1)}, u32[]{:S(2)}, u32[]{:S(2)}) collective-permute-start(bf16[128,512]{1,0:T(8,128)(2,1)S(1)} %constant_dynamic-update-slice_fusion), channel_id=1, source_target_pairs={{0,64},{32,96},{64,0},{96,32},{1,65},{33,97},{65,1},{97,33},{2,66}... | collective-permute-start | bytes 393224 | tf_op jit(solution)/shard_map/ppermute | solution.py:291
  19.9 24.7 %collective-permute-start = (bf16[128,512]{1,0:T(8,128)(2,1)S(1)}, bf16[128,512]{1,0:T(8,128)(2,1)S(1)}, u32[]{:S(2)}, u32[]{:S(2)}) collective-permute-start(bf16[128,512]{1,0:T(8,128)(2,1)S(1)} %constant_dynamic-update-slice_fusion), channel_id=1, source_target_pairs={{0,96},{32,0},{64,32},{96,64},{1,97},{33,1},{65,33},{97,65},{2,98}... | collective-permute-start | bytes 393224 | tf_op jit(solution)/shard_map/ppermute | solution.py:291
  25.6 24.7 %all-to-all-start = ((bf16[4,16,128]{2,1,0:T(8,128)(2,1)}), bf16[4,16,128]{2,1,0:T(8,128)(2,1)S(1)}, u32[]{:S(2)}, u32[]{:S(2)}) async-start(bf16[4,16,128]{2,1,0:T(8,128)(2,1)} %bitcast.33), calls=%async_computation | async-start | bytes 32768 | tf_op jit(solution)/shard_map/all_to_all | solution.py:18
  44.6 19.8 %collective-permute-start.3 = (bf16[512,512]{1,0:T(8,128)(2,1)S(1)}, bf16[512,512]{1,0:T(8,128)(2,1)S(1)}, u32[]{:S(2)}, u32[]{:S(2)}) collective-permute-start(bf16[512,512]{1,0:T(8,128)(2,1)S(1)} %pad_maximum_fusion.mine_ref), channel_id=1, source_target_pairs={{0,16},{16,0},{1,17},{17,1},{2,18},{18,2},{3,19},{19,3},{4,20},{20... | collective-permute-start | bytes 1572872 | tf_op jit(solution)/shard_map/ppermute | solution.py:245
  65.5 25.5 %all-to-all-start.2 = ((bf16[4,32,512]{2,1,0:T(8,128)(2,1)}), bf16[4,32,512]{2,1,0:T(8,128)(2,1)S(1)}, u32[]{:S(2)}, u32[]{:S(2)}) async-start(bf16[4,32,512]{2,1,0:T(8,128)(2,1)} %shard_map.220), calls=%async_computation.2 | async-start | bytes 262144 | tf_op jit(solution)/shard_map/all_to_all | solution.py:18
Sparse Core Ops, SparseCore 0:
  10.7 81.9 all-gather.2
